TPU v7x, 512 devices: a whole 4x4x16 slice. The times are simulated.
512 devices in a mesh: sp: 32 (over z, core), tp: 16 (over y, x).
Axes of the slice: x: 4, y: 4, z: 16, core: 2. Of those that a mesh axis runs over, the one named last changes fastest.
Arguments:
- resid: bfloat16 [65536, 2048], P(('sp', 'tp')), may hold values from -6 to 6
- branch_input: bfloat16 [1024, 65536], P('tp', 'sp'), may hold values from -6 to 6
- gate_in: bfloat16 [1024, 65536], P('tp', 'sp'), may hold values from -6 to 6
- conv_taps: bfloat16 [4, 1024], P(None, 'tp'), may hold values from -3 to 3
- rate_weight: bfloat16 [16, 64, 64], P('tp'), may hold values from -0.75 to 0.75
- input_weight: bfloat16 [16, 64, 64], P('tp'), may hold values from -0.75 to 0.75
- decay_base: float32 [1024], P('tp')
- decay_extra: float32 [65536], P('sp'), may hold values from -2 to 0
- out_weight: bfloat16 [1024, 2048], P('tp'), may hold values from -0.1875 to 0.1875
- gain_mix: float32 [2048], replicated, may hold values from 0.1 to 1.9
- gain_pre: float32 [2048], replicated, may hold values from 0.1 to 1.9
- gain_post: float32 [2048], replicated, may hold values from 0.1 to 1.9
- expert_ids: int32 [65536, 2], P(('sp', 'tp')), may hold values from 0 to 31, as said below
- route_weight: float32 [65536, 2], P(('sp', 'tp')), may hold values from 0.2 to 1
- gate_proj: bfloat16 [32, 512, 2048], P('sp', 'tp'), may hold values from -0.125 to 0.125
- up_proj: bfloat16 [32, 512, 2048], P('sp', 'tp'), may hold values from -0.125 to 0.125
- down_proj: bfloat16 [32, 512, 2048], P('sp', 'tp'), may hold values from -0.25 to 0.25
Outputs:
- layer_out: bfloat16 [65536, 2048], P(('sp', 'tp'))
Inputs may be any that keep to these rules, and one draw needn't show every extreme that they name: `expert_ids`: each row names two different experts of one group: both lie in g * 8 .. g * 8 + 7 for some g. In each aligned block of 128 rows (the rows of one device) every expert is named by exactly 8 rows.
All inputs are finite; a program needn't handle non-finite values.
Results may differ from a plain program's by a relative error of at most 0.0065.
Values may be sent and summed in bfloat16 or wider, within the bound.
A program may use at most 128 MiB of HBM per device.

v0:
```python
import math

import jax
import jax.numpy as jnp
from jax import lax
from jax.sharding import Mesh
from jax.sharding import PartitionSpec as P

SP = ("sp_0", "sp_1")
SP_TP = ("sp_0", "sp_1", "tp")


epsilon = 1e-06
gate_power = 8.0


def sent_to_all(array, axis):
    count = lax.axis_size(axis)
    return lax.all_to_all(
        jnp.broadcast_to(array[None], (count, *array.shape)), axis, 0, 0, tiled=True
    )


def gathered_once(array, axis):
    leaves = jax.tree.leaves(array)
    order = sorted(range(len(leaves)), key=lambda k: -leaves[k].size)
    width = (1, *leaves[order[0]].shape)[-1]
    lines = [
        jnp.pad(leaves[k].reshape(-1), (0, -leaves[k].size % width)).reshape(-1, width)
        for k in order
    ]
    both, at, found = (sent_to_all(jnp.concatenate(lines), axis), 0, {})
    for k, line in zip(order, lines):
        section = both[:, at : at + len(line)].reshape(len(both), -1)
        found[k] = section[:, : leaves[k].size].reshape(-1, *leaves[k].shape)
        at += len(line)
    numbers = iter(range(len(leaves)))
    return jax.tree.map(lambda _: found[next(numbers)], array)


def folded_in_pairs(pieces, combine):
    while len(jax.tree.leaves(pieces)[0]) > 1:
        pieces = jax.vmap(combine)(
            *(jax.tree.map(lambda part: part[side::2], pieces) for side in (0, 1))
        )
    return jax.tree.map(lambda part: part[0], pieces)


def prefix(array, axis, combine, identity):
    count, here = (lax.axis_size(axis), lax.axis_index(axis))
    passed = jnp.arange(count) < here

    def kept(part, zero, own):
        part = jnp.where(
            passed.reshape(-1, *(1 for _ in own.shape)), part, jnp.asarray(zero, own.dtype)
        )
        return part

    pieces = gathered_once(array, axis)
    return folded_in_pairs(jax.tree.map(kept, pieces, identity, array), combine)


def in_one_piece(arrays, axis, dim, along):
    widths = [a.shape[along] for a in arrays]
    both = jnp.concatenate(arrays, axis=along)
    out = lax.all_gather(both, axis, axis=dim, tiled=True)
    return tuple(jnp.split(out, [sum(widths[:k]) for k in range(1, len(widths))], axis=along))


def passed_along(value, axis, steps):
    count = lax.axis_size(axis)
    first, last = (max(0, -steps), min(count, count - steps))
    return lax.ppermute(value, axis, [(source, source + steps) for source in range(first, last)])


def cut_along(array, dim, count):
    before, after = (array.shape[:dim], array.shape[dim + 1 :])
    return jnp.moveaxis(array.reshape(*before, count, -1, *after), dim, 0)


def joined_along(tiles, dim):
    tiles = jnp.moveaxis(tiles, 0, dim)
    dims = tiles.shape
    return tiles.reshape(*dims[:dim], dims[dim] * dims[dim + 1], *dims[dim + 2 :])


def moved_by_axis(tiles, axes, order):
    dims = [lax.axis_size(a) for a in axes]
    tiles = tiles.reshape(*dims, *tiles.shape[1:])
    for k in order:
        tiles = lax.all_to_all(tiles, axes[k], split_axis=k, concat_axis=k, tiled=True)
    return tiles.reshape(-1, *tiles.shape[len(axes) :])


def exchange_by_chip(array, groups, order, split_dim, concat_dim):
    count = lax.axis_size(groups[0]) * lax.axis_size(groups[1])
    tiles = cut_along(array, split_dim, count)
    return joined_along(moved_by_axis(tiles, groups, order), concat_dim)


def normalized(values, gain):
    return values * lax.rsqrt(jnp.mean(values * values, axis=-1, keepdims=True) + epsilon) * gain


def combine_pair(earlier, latter):
    return (earlier[0] * latter[0], latter[0] * earlier[1] + latter[1])


def carry_in(block_keep, block_state):
    identity = (jnp.ones(block_keep.shape, jnp.float32), jnp.zeros(block_state.shape, jnp.float32))
    return prefix((block_keep, block_state), SP, combine_pair, identity)


def block_recurrence(log_keep, driven, start_state):
    channels, positions = log_keep.shape
    span = math.gcd(positions, 128)
    count = positions // span
    order = jnp.arange(span, dtype=jnp.int32)
    lower = (order[:, None] >= order[None, :])[None, :, :]

    def one_block(index, carried):
        state, total_log, states_out, logs_out = carried
        first = index * span
        block_log = lax.dynamic_slice_in_dim(log_keep, first, span, 1)
        block_drive = lax.dynamic_slice_in_dim(driven, first, span, 1)
        running = jnp.cumsum(block_log, axis=1)
        gap = jnp.where(lower, running[:, :, None] - running[:, None, :], -jnp.inf)
        inner = jnp.einsum("cts,cs->ct", jnp.exp(gap), block_drive, precision=lax.Precision.HIGHEST)
        produced = inner + jnp.exp(running) * state[:, None]
        whole_log = running + total_log[:, None]
        states_out = lax.dynamic_update_slice_in_dim(states_out, produced, first, 1)
        logs_out = lax.dynamic_update_slice_in_dim(logs_out, whole_log, first, 1)
        return (produced[:, -1], whole_log[:, -1], states_out, logs_out)

    initial = (
        start_state,
        jnp.zeros((channels,), jnp.float32),
        jnp.zeros((channels, positions), jnp.float32),
        jnp.zeros((channels, positions), jnp.float32),
    )
    _, _, hidden_state, summed_log = lax.fori_loop(0, count, one_block, initial)
    return (hidden_state, summed_log)


def per_device(
    resid,
    branch_input,
    gate_in,
    conv_taps,
    rate_weight,
    input_weight,
    decay_base,
    decay_extra,
    out_weight,
    gain_mix,
    gain_pre,
    gain_post,
    expert_ids,
    route_weight,
    gate_proj,
    up_proj,
    down_proj,
):
    channels, positions = branch_input.shape
    tap_count = conv_taps.shape[0]
    fetched = (
        lax.all_gather(out_weight, "tp", axis=0, tiled=True),
        *in_one_piece((gate_proj, up_proj, down_proj), "tp", 1, 0),
    )
    edge_cols = passed_along(branch_input[:, positions - (tap_count - 1) :], SP, 1)
    padded = jnp.concatenate([edge_cols, branch_input], axis=1).astype(jnp.float32)
    filter_tap_weights = conv_taps.astype(jnp.float32)
    convolved = filter_tap_weights[0][:, None] * padded[:, 0:positions]
    for offset in range(1, tap_count):
        convolved = (
            convolved + filter_tap_weights[offset][:, None] * padded[:, offset : offset + positions]
        )
    grouped = convolved.reshape(rate_weight.shape[0], rate_weight.shape[1], positions)
    rate_gate = jax.nn.sigmoid(
        jnp.einsum(
            "ncs,ncd->nds",
            grouped,
            rate_weight.astype(jnp.float32),
            precision=lax.Precision.HIGHEST,
        ).reshape(channels, positions)
    )
    input_gate = jax.nn.sigmoid(
        jnp.einsum(
            "ncs,ncd->nds",
            grouped,
            input_weight.astype(jnp.float32),
            precision=lax.Precision.HIGHEST,
        ).reshape(channels, positions)
    )
    decay_rate = -gate_power * jax.nn.softplus(-decay_base)
    log_keep = decay_rate[:, None] * rate_gate + decay_extra[None, :]
    driven = jnp.sqrt(-jnp.expm1(2.0 * log_keep)) * input_gate * convolved
    zero_state = jnp.zeros((channels,), jnp.float32)
    local_state, summed_log = block_recurrence(log_keep, driven, zero_state)
    retained = jnp.exp(summed_log)
    _, entering = carry_in(retained[:, -1], local_state[:, -1])
    hidden_state = local_state + retained * entering[:, None]
    branch_out = (hidden_state * jax.nn.gelu(gate_in.astype(jnp.float32), approximate=True)).astype(
        jnp.bfloat16
    )
    token_rows = lax.all_to_all(branch_out, "tp", split_axis=1, concat_axis=0, tiled=True)
    token_count = token_rows.shape[1]
    mixed_rows = lax.dot_general(
        token_rows, fetched[0], (((0,), (0,)), ((), ())), preferred_element_type=jnp.float32
    )
    after_mix = resid.astype(jnp.float32) + normalized(mixed_rows, gain_mix)
    ffn_in = normalized(after_mix, gain_pre).astype(jnp.bfloat16)
    top_count = expert_ids.shape[1]
    experts = gate_proj.shape[0] * lax.axis_size(SP)
    capacity = top_count * token_count // experts
    chosen = expert_ids.reshape(-1)
    matches = (chosen[:, None] == jnp.arange(experts, dtype=jnp.int32)[None, :]).astype(jnp.int32)
    slot_index = jnp.sum((jnp.cumsum(matches, axis=0) - 1) * matches, axis=1)
    target = chosen * capacity + slot_index
    source = (
        jnp.zeros((experts * capacity,), jnp.int32)
        .at[target]
        .set(jnp.arange(token_count * top_count, dtype=jnp.int32) // top_count)
    )
    outgoing = ffn_in[source].reshape(experts, capacity, ffn_in.shape[1])
    arriving = lax.all_to_all(outgoing, SP, split_axis=0, concat_axis=1, tiled=True)
    gate_rows = fetched[1]
    up_rows = fetched[2]
    down_rows = fetched[3]
    gate_vals = jnp.einsum("emd,ekd->emk", arriving, gate_rows, preferred_element_type=jnp.float32)
    up_vals = jnp.einsum("emd,ekd->emk", arriving, up_rows, preferred_element_type=jnp.float32)
    hidden = (jax.nn.silu(gate_vals) * up_vals).astype(jnp.bfloat16)
    result = jnp.einsum("emk,ekd->emd", hidden, down_rows, preferred_element_type=jnp.float32)
    returned = exchange_by_chip(result.astype(jnp.bfloat16), ("sp_0", "sp_1"), (1, 0), 1, 0)
    returned = returned.reshape(experts * capacity, returned.shape[2])
    picked = returned[target].astype(jnp.float32).reshape(token_count, top_count, returned.shape[1])
    moe = jnp.sum(picked * route_weight[:, :, None], axis=1)
    return (after_mix + normalized(moe, gain_post)).astype(jnp.bfloat16)


def solution(mesh):
    split = Mesh(mesh.devices.reshape(16, 2, mesh.shape["tp"]), ("sp_0", "sp_1", "tp"))
    return jax.shard_map(
        per_device,
        mesh=split,
        in_specs=(
            P(SP_TP, None),
            P("tp", SP),
            P("tp", SP),
            P(None, "tp"),
            P("tp", None, None),
            P("tp", None, None),
            P("tp"),
            P(SP),
            P("tp", None),
            P(),
            P(),
            P(),
            P(SP_TP, None),
            P(SP_TP, None),
            P(SP, "tp", None),
            P(SP, "tp", None),
            P(SP, "tp", None),
        ),
        out_specs=P(SP_TP, None),
        check_vma=False,
    )
```

profile of v0, /device:TPU:1, one launch (start us, length us, event | category | flops | bytes accessed | tf_op | source)
XLA Modules:
  0.0 340.2 jit_solution(10966151142271270627)
XLA Ops:
  6.5 0.7 all-gather.3.cloned.1.call-update
  7.3 0.8 slice.120
  8.1 4.9 %collective-permute-start = (bf16[64,3]{1,0:T(8,128)(2,1)S(1)}, bf16[64,3]{1,0:T(8,128)(2,1)S(1)}, u32[]{:S(2)}, u32[]{:S(2)}) collective-permute-start(bf16[64,3]{1,0:T(8,128)(2,1)S(1)} %slice.120), channel_id=1, source_target_pairs={{0,16},{16,32},{32,48},{48,64},{64,80},{80,96},{96,112},{112,128},... | collective-permute-start | bytes 1160 | tf_op jit(solution)/shard_map/ppermute | solution.py:73
  13.0 1.8 pad_maximum_fusion
  14.9 0.8 copy.33
  15.9 0.7 broadcast_multiply_fusion
  16.6 0.7 convert_element_type.44
  19.2 1.4 scatter_custom_fusion
  20.6 1.1 maximum_convert_fusion
  22.8 0.7 fusion.23
  23.6 124.2 %while.20 = (s32[]{:T(128)}, f32[64]{0:T(128)S(1)}, f32[64]{0:T(128)S(1)}, f32[64,2048]{1,0:T(8,128)S(1)}, f32[64,2048]{1,0:T(8,128)S(1)}, /*index=5*/f32[64,204...) while((s32[]{:T(128)}, f32[64]{0:T(128)S(1)}, ...), condition=%wide.region_2.3_spmd.clone, body=%wide.region_0.2_spmd.clone.sunk | while | flops 15761414 | bytes 526511 | solution.py:141
  24.0 6.9 %fusion.75 = f32[64,1,128]{2,1,0:T(1,128)S(1)} fusion(f32[64,128,1]{1,2,0:T(1,128)S(1)} %bitcast.103, f32[64,128]{1,0:T(8,128)S(1)} %reduce_window_sum.33, pred[128,128]{1,0:T(8,128)(4,1)S(1)} %fusion.74), kind=kOutput, calls=%fused_computation.4.clone.1 | convolution fusion | flops 14680064 | bytes 114688 | tf_op jit(solution)/shard_map/while/body/eval_jaxpr/cts,cs->ct/dot_general | solution.py:128
  31.7 6.9 %fusion.75 = f32[64,1,128]{2,1,0:T(1,128)S(1)} fusion(f32[64,128,1]{1,2,0:T(1,128)S(1)} %bitcast.103, f32[64,128]{1,0:T(8,128)S(1)} %reduce_window_sum.33, pred[128,128]{1,0:T(8,128)(4,1)S(1)} %fusion.74), kind=kOutput, calls=%fused_computation.4.clone.1 | convolution fusion | flops 14680064 | bytes 114688 | tf_op jit(solution)/shard_map/while/body/eval_jaxpr/cts,cs->ct/dot_general | solution.py:128
  39.5 6.9 %fusion.75 = f32[64,1,128]{2,1,0:T(1,128)S(1)} fusion(f32[64,128,1]{1,2,0:T(1,128)S(1)} %bitcast.103, f32[64,128]{1,0:T(8,128)S(1)} %reduce_window_sum.33, pred[128,128]{1,0:T(8,128)(4,1)S(1)} %fusion.74), kind=kOutput, calls=%fused_computation.4.clone.1 | convolution fusion | flops 14680064 | bytes 114688 | tf_op jit(solution)/shard_map/while/body/eval_jaxpr/cts,cs->ct/dot_general | solution.py:128
  47.3 6.9 %fusion.75 = f32[64,1,128]{2,1,0:T(1,128)S(1)} fusion(f32[64,128,1]{1,2,0:T(1,128)S(1)} %bitcast.103, f32[64,128]{1,0:T(8,128)S(1)} %reduce_window_sum.33, pred[128,128]{1,0:T(8,128)(4,1)S(1)} %fusion.74), kind=kOutput, calls=%fused_computation.4.clone.1 | convolution fusion | flops 14680064 | bytes 114688 | tf_op jit(solution)/shard_map/while/body/eval_jaxpr/cts,cs->ct/dot_general | solution.py:128
  55.0 6.9 %fusion.75 = f32[64,1,128]{2,1,0:T(1,128)S(1)} fusion(f32[64,128,1]{1,2,0:T(1,128)S(1)} %bitcast.103, f32[64,128]{1,0:T(8,128)S(1)} %reduce_window_sum.33, pred[128,128]{1,0:T(8,128)(4,1)S(1)} %fusion.74), kind=kOutput, calls=%fused_computation.4.clone.1 | convolution fusion | flops 14680064 | bytes 114688 | tf_op jit(solution)/shard_map/while/body/eval_jaxpr/cts,cs->ct/dot_general | solution.py:128
  62.8 6.9 %fusion.75 = f32[64,1,128]{2,1,0:T(1,128)S(1)} fusion(f32[64,128,1]{1,2,0:T(1,128)S(1)} %bitcast.103, f32[64,128]{1,0:T(8,128)S(1)} %reduce_window_sum.33, pred[128,128]{1,0:T(8,128)(4,1)S(1)} %fusion.74), kind=kOutput, calls=%fused_computation.4.clone.1 | convolution fusion | flops 14680064 | bytes 114688 | tf_op jit(solution)/shard_map/while/body/eval_jaxpr/cts,cs->ct/dot_general | solution.py:128
  70.6 6.9 %fusion.75 = f32[64,1,128]{2,1,0:T(1,128)S(1)} fusion(f32[64,128,1]{1,2,0:T(1,128)S(1)} %bitcast.103, f32[64,128]{1,0:T(8,128)S(1)} %reduce_window_sum.33, pred[128,128]{1,0:T(8,128)(4,1)S(1)} %fusion.74), kind=kOutput, calls=%fused_computation.4.clone.1 | convolution fusion | flops 14680064 | bytes 114688 | tf_op jit(solution)/shard_map/while/body/eval_jaxpr/cts,cs->ct/dot_general | solution.py:128
  78.3 6.9 %fusion.75 = f32[64,1,128]{2,1,0:T(1,128)S(1)} fusion(f32[64,128,1]{1,2,0:T(1,128)S(1)} %bitcast.103, f32[64,128]{1,0:T(8,128)S(1)} %reduce_window_sum.33, pred[128,128]{1,0:T(8,128)(4,1)S(1)} %fusion.74), kind=kOutput, calls=%fused_computation.4.clone.1 | convolution fusion | flops 14680064 | bytes 114688 | tf_op jit(solution)/shard_map/while/body/eval_jaxpr/cts,cs->ct/dot_general | solution.py:128
  86.1 6.9 %fusion.75 = f32[64,1,128]{2,1,0:T(1,128)S(1)} fusion(f32[64,128,1]{1,2,0:T(1,128)S(1)} %bitcast.103, f32[64,128]{1,0:T(8,128)S(1)} %reduce_window_sum.33, pred[128,128]{1,0:T(8,128)(4,1)S(1)} %fusion.74), kind=kOutput, calls=%fused_computation.4.clone.1 | convolution fusion | flops 14680064 | bytes 114688 | tf_op jit(solution)/shard_map/while/body/eval_jaxpr/cts,cs->ct/dot_general | solution.py:128
  93.8 6.9 %fusion.75 = f32[64,1,128]{2,1,0:T(1,128)S(1)} fusion(f32[64,128,1]{1,2,0:T(1,128)S(1)} %bitcast.103, f32[64,128]{1,0:T(8,128)S(1)} %reduce_window_sum.33, pred[128,128]{1,0:T(8,128)(4,1)S(1)} %fusion.74), kind=kOutput, calls=%fused_computation.4.clone.1 | convolution fusion | flops 14680064 | bytes 114688 | tf_op jit(solution)/shard_map/while/body/eval_jaxpr/cts,cs->ct/dot_general | solution.py:128
  101.6 6.9 %fusion.75 = f32[64,1,128]{2,1,0:T(1,128)S(1)} fusion(f32[64,128,1]{1,2,0:T(1,128)S(1)} %bitcast.103, f32[64,128]{1,0:T(8,128)S(1)} %reduce_window_sum.33, pred[128,128]{1,0:T(8,128)(4,1)S(1)} %fusion.74), kind=kOutput, calls=%fused_computation.4.clone.1 | convolution fusion | flops 14680064 | bytes 114688 | tf_op jit(solution)/shard_map/while/body/eval_jaxpr/cts,cs->ct/dot_general | solution.py:128
  109.4 6.9 %fusion.75 = f32[64,1,128]{2,1,0:T(1,128)S(1)} fusion(f32[64,128,1]{1,2,0:T(1,128)S(1)} %bitcast.103, f32[64,128]{1,0:T(8,128)S(1)} %reduce_window_sum.33, pred[128,128]{1,0:T(8,128)(4,1)S(1)} %fusion.74), kind=kOutput, calls=%fused_computation.4.clone.1 | convolution fusion | flops 14680064 | bytes 114688 | tf_op jit(solution)/shard_map/while/body/eval_jaxpr/cts,cs->ct/dot_general | solution.py:128
  117.1 6.9 %fusion.75 = f32[64,1,128]{2,1,0:T(1,128)S(1)} fusion(f32[64,128,1]{1,2,0:T(1,128)S(1)} %bitcast.103, f32[64,128]{1,0:T(8,128)S(1)} %reduce_window_sum.33, pred[128,128]{1,0:T(8,128)(4,1)S(1)} %fusion.74), kind=kOutput, calls=%fused_computation.4.clone.1 | convolution fusion | flops 14680064 | bytes 114688 | tf_op jit(solution)/shard_map/while/body/eval_jaxpr/cts,cs->ct/dot_general | solution.py:128
  124.9 6.9 %fusion.75 = f32[64,1,128]{2,1,0:T(1,128)S(1)} fusion(f32[64,128,1]{1,2,0:T(1,128)S(1)} %bitcast.103, f32[64,128]{1,0:T(8,128)S(1)} %reduce_window_sum.33, pred[128,128]{1,0:T(8,128)(4,1)S(1)} %fusion.74), kind=kOutput, calls=%fused_computation.4.clone.1 | convolution fusion | flops 14680064 | bytes 114688 | tf_op jit(solution)/shard_map/while/body/eval_jaxpr/cts,cs->ct/dot_general | solution.py:128
  132.7 6.9 %fusion.75 = f32[64,1,128]{2,1,0:T(1,128)S(1)} fusion(f32[64,128,1]{1,2,0:T(1,128)S(1)} %bitcast.103, f32[64,128]{1,0:T(8,128)S(1)} %reduce_window_sum.33, pred[128,128]{1,0:T(8,128)(4,1)S(1)} %fusion.74), kind=kOutput, calls=%fused_computation.4.clone.1 | convolution fusion | flops 14680064 | bytes 114688 | tf_op jit(solution)/shard_map/while/body/eval_jaxpr/cts,cs->ct/dot_general | solution.py:128
  140.4 6.9 %fusion.75 = f32[64,1,128]{2,1,0:T(1,128)S(1)} fusion(f32[64,128,1]{1,2,0:T(1,128)S(1)} %bitcast.103, f32[64,128]{1,0:T(8,128)S(1)} %reduce_window_sum.33, pred[128,128]{1,0:T(8,128)(4,1)S(1)} %fusion.74), kind=kOutput, calls=%fused_computation.4.clone.1 | convolution fusion | flops 14680064 | bytes 114688 | tf_op jit(solution)/shard_map/while/body/eval_jaxpr/cts,cs->ct/dot_general | solution.py:128
  148.3 0.7 reshape.230
  149.0 14.5 %all-to-all-start = ((f32[32,1,128]{2,1,0:T(1,128)}), f32[32,1,128]{2,1,0:T(1,128)S(1)}, u32[]{:S(2)}, u32[]{:S(2)}) async-start(f32[32,1,128]{2,1,0:T(1,128)} %reshape.230), calls=%async_computation | async-start | bytes 32768 | tf_op jit(solution)/shard_map/all_to_all | solution.py:19
  163.5 11.8 %all-to-all-done = f32[32,1,128]{2,1,0:T(1,128)S(1)} async-done(((f32[32,1,128]{2,1,0:T(1,128)}), f32[32,1,128]{2,1,0:T(1,128)S(1)}, u32[]{:S(2)}, u32[]{:S(2)}) %all-to-all-start) | async-done | bytes 16416 | tf_op jit(solution)/shard_map/all_to_all | solution.py:19
  175.9 0.7 reduce.10
  177.1 1.0 copy_bitcast_fusion
  178.1 6.9 %all-to-all-start.1 = ((bf16[64,16,128]{2,0,1:T(8,128)(2,1)}), bf16[64,16,128]{2,0,1:T(8,128)(2,1)S(1)}, u32[]{:S(2)}, u32[]{:S(2)}) async-start(bf16[64,16,128]{2,0,1:T(8,128)(2,1)} %copy_bitcast_fusion), calls=%async_computation.1 | async-start | bytes 524288 | tf_op jit(solution)/shard_map/all_to_all | solution.py:206
  185.1 7.6 %all-to-all-done.1 = bf16[64,16,128]{2,0,1:T(8,128)(2,1)S(1)} async-done(((bf16[64,16,128]{2,0,1:T(8,128)(2,1)}), bf16[64,16,128]{2,0,1:T(8,128)(2,1)S(1)}, u32[]{:S(2)}, u32[]{:S(2)}) %all-to-all-start.1) | async-done | bytes 262176 | tf_op jit(solution)/shard_map/all_to_all | solution.py:206
  192.7 3.0 multiply_reduce_fusion.3
  196.4 2.4 gather_fusion
  198.8 5.8 %all-to-all-start.2 = ((bf16[32,8,2048]{2,1,0:T(8,128)(2,1)}), bf16[32,8,2048]{2,1,0:T(8,128)(2,1)S(1)}, u32[]{:S(2)}, u32[]{:S(2)}) async-start(bf16[32,8,2048]{2,1,0:T(8,128)(2,1)} %bitcast.16), calls=%async_computation.2 | async-start | bytes 2097152 | tf_op jit(solution)/shard_map/all_to_all | solution.py:226
  204.7 55.7 %all-to-all-done.2 = bf16[32,8,2048]{2,1,0:T(8,128)(2,1)S(1)} async-done(((bf16[32,8,2048]{2,1,0:T(8,128)(2,1)}), bf16[32,8,2048]{2,1,0:T(8,128)(2,1)S(1)}, u32[]{:S(2)}, u32[]{:S(2)}) %all-to-all-start.2) | async-done | bytes 1048608 | tf_op jit(solution)/shard_map/all_to_all | solution.py:226
  260.4 3.1 fusion.25
  263.5 3.8 %convolution_convert_fusion = bf16[256,2048]{1,0:T(8,128)(2,1)S(1)} fusion(bf16[3,512,2048]{2,1,0:T(8,128)(2,1)} %all-gather.5.cloned.1.call-done, bf16[32,8,2048]{2,1,0:T(8,128)(2,1)S(1)} %all-to-all-done.2, f32[256,512]{1,0:T(8,128)} %fusion.25), kind=kOutput, calls=%fused_computation.23 | convolution fusion | flops 1075052544 | bytes 6815744 | tf_op jit(solution)/shard_map/emk,ekd->emd/dot_general | solution.py:233
  267.4 5.3 %all_to_all.43 = bf16[16,2,1,8,2048]{4,3,0,2,1:T(8,128)(2,1)S(1)} all-to-all(bf16[16,2,1,8,2048]{4,3,0,2,1:T(8,128)(2,1)S(1)} %copy.36), channel_id=1, replica_groups=mesh['sp_0'=16,'sp_1'=2,'tp'=16] {'sp_1'}, dimensions={1} | all-to-all | bytes 2097152 | tf_op jit(solution)/shard_map/all_to_all | solution.py:91
  272.7 1.1 copy.37
  273.8 3.7 %all-to-all-start.4 = ((bf16[16,2,1,8,2048]{4,3,1,2,0:T(8,128)(2,1)}), bf16[16,2,1,8,2048]{4,3,1,2,0:T(8,128)(2,1)S(1)}, u32[]{:S(2)}, u32[]{:S(2)}) async-start(bf16[16,2,1,8,2048]{4,3,1,2,0:T(8,128)(2,1)} %copy.37), calls=%async_computation.4 | async-start | bytes 2097152 | tf_op jit(solution)/shard_map/all_to_all | solution.py:91
  277.5 46.6 %all-to-all-done.4 = bf16[16,2,1,8,2048]{4,3,1,2,0:T(8,128)(2,1)S(1)} async-done(((bf16[16,2,1,8,2048]{4,3,1,2,0:T(8,128)(2,1)}), bf16[16,2,1,8,2048]{4,3,1,2,0:T(8,128)(2,1)S(1)}, u32[]{:S(2)}, u32[]{:S(2)}) %all-to-all-start.4) | async-done | bytes 1048608 | tf_op jit(solution)/shard_map/all_to_all | solution.py:91
  324.1 2.3 gather_fusion.1
  326.5 2.4 reshape.195
  328.9 3.1 multiply_reduce_fusion
  332.1 1.2 add_convert_fusion
  (184 shorter events, 18.4 us)
Async XLA Ops:
  6.5 15.7 %copy-start = (bf16[1,64,64]{2,1,0:T(8,128)(2,1)S(1)}, bf16[1,64,64]{2,1,0:T(8,128)(2,1)}, u32[]{:S(2)}) copy-start(bf16[1,64,64]{2,1,0:T(8,128)(2,1)} %param.23) | copy-start | bytes 24580
  6.5 15.7 %copy-start.9 = (f32[2048]{0:T(1024)S(1)}, f32[2048]{0:T(1024)}, u32[]{:S(2)}) copy-start(f32[2048]{0:T(1024)} %param.26) | copy-start | bytes 24580
  6.5 16.2 %copy-start.8 = (bf16[1,64,64]{2,1,0:T(8,128)(2,1)S(1)}, bf16[1,64,64]{2,1,0:T(8,128)(2,1)}, u32[]{:S(2)}) copy-start(bf16[1,64,64]{2,1,0:T(8,128)(2,1)} %param.24) | copy-start | bytes 24580
  6.5 186.1 %all-gather.3.cloned.1.call-start = ((), (), s32[]{:S(2)}) async-start(), calls=%async_computation.5 | async-start | bytes 4456448 | tf_op jit(solution)/shard_map/all_gather | solution.py:167
  7.3 197.4 %all-gather.5.cloned.1.call-start = ((), (), s32[]{:S(2)}) async-start(), calls=%async_computation.6 | async-start | bytes 6684672 | tf_op jit(solution)/shard_map/all_gather | solution.py:66
  8.1 12.5 %collective-permute-start = (bf16[64,3]{1,0:T(8,128)(2,1)S(1)}, bf16[64,3]{1,0:T(8,128)(2,1)S(1)}, u32[]{:S(2)}, u32[]{:S(2)}) collective-permute-start(bf16[64,3]{1,0:T(8,128)(2,1)S(1)} %slice.120), channel_id=1, source_target_pairs={{0,16},{16,32},{32,48},{48,64},{64,80},{80,96},{96,112},{112,128},... | collective-permute-start | bytes 1160 | tf_op jit(solution)/shard_map/ppermute | solution.py:73
  23.6 153.5 %copy-start.3 = (bf16[64,2048]{1,0:T(8,128)(2,1)S(1)}, bf16[64,2048]{1,0:T(8,128)(2,1)}, u32[]{:S(2)}) copy-start(bf16[64,2048]{1,0:T(8,128)(2,1)} %param.21) | copy-start | bytes 786436
  147.9 47.8 %copy-start.1 = (bf16[128,2048]{1,0:T(8,128)(2,1)S(1)}, bf16[128,2048]{1,0:T(8,128)(2,1)}, u32[]{:S(2)}) copy-start(bf16[128,2048]{1,0:T(8,128)(2,1)} %param.19) | copy-start | bytes 1572868
  147.9 47.8 %copy-start.4 = (f32[2048]{0:T(1024)S(1)}, f32[2048]{0:T(1024)}, u32[]{:S(2)}) copy-start(f32[2048]{0:T(1024)} %param.28) | copy-start | bytes 24580
  149.0 26.2 %all-to-all-start = ((f32[32,1,128]{2,1,0:T(1,128)}), f32[32,1,128]{2,1,0:T(1,128)S(1)}, u32[]{:S(2)}, u32[]{:S(2)}) async-start(f32[32,1,128]{2,1,0:T(1,128)} %reshape.230), calls=%async_computation | async-start | bytes 32768 | tf_op jit(solution)/shard_map/all_to_all | solution.py:19
  178.1 18.0 %copy-start.5 = (f32[2048]{0:T(1024)S(1)}, f32[2048]{0:T(1024)}, u32[]{:S(2)}) copy-start(f32[2048]{0:T(1024)} %param.29) | copy-start | bytes 24580
  178.1 14.6 %all-to-all-start.1 = ((bf16[64,16,128]{2,0,1:T(8,128)(2,1)}), bf16[64,16,128]{2,0,1:T(8,128)(2,1)S(1)}, u32[]{:S(2)}, u32[]{:S(2)}) async-start(bf16[64,16,128]{2,0,1:T(8,128)(2,1)} %copy_bitcast_fusion), calls=%async_computation.1 | async-start | bytes 524288 | tf_op jit(solution)/shard_map/all_to_all | solution.py:206
  198.8 61.6 %all-to-all-start.2 = ((bf16[32,8,2048]{2,1,0:T(8,128)(2,1)}), bf16[32,8,2048]{2,1,0:T(8,128)(2,1)S(1)}, u32[]{:S(2)}, u32[]{:S(2)}) async-start(bf16[32,8,2048]{2,1,0:T(8,128)(2,1)} %bitcast.16), calls=%async_computation.2 | async-start | bytes 2097152 | tf_op jit(solution)/shard_map/all_to_all | solution.py:226
  267.3 10.1 %copy-start.7 = (f32[128,2]{0,1:T(2,128)S(1)}, f32[128,2]{0,1:T(2,128)}, u32[]{:S(2)}) copy-start(f32[128,2]{0,1:T(2,128)} %param.32) | copy-start | bytes 3076
  273.8 50.4 %all-to-all-start.4 = ((bf16[16,2,1,8,2048]{4,3,1,2,0:T(8,128)(2,1)}), bf16[16,2,1,8,2048]{4,3,1,2,0:T(8,128)(2,1)S(1)}, u32[]{:S(2)}, u32[]{:S(2)}) async-start(bf16[16,2,1,8,2048]{4,3,1,2,0:T(8,128)(2,1)} %copy.37), calls=%async_computation.4 | async-start | bytes 2097152 | tf_op jit(solution)/shard_map/all_to_all | solution.py:91
  326.5 5.7 %copy-start.6 = (f32[2048]{0:T(1024)S(1)}, f32[2048]{0:T(1024)}, u32[]{:S(2)}) copy-start(f32[2048]{0:T(1024)} %param.30) | copy-start | bytes 24580
  328.8 3.3 copy-start.2
Sparse Core Ops, SparseCore 0:
  10.3 71.8 all-gather.2
  85.2 76.2 all-gather.4
where the time goes:
time: 343 us; the launch traced here: 340 us
  waiting for transfers between devices  122 us (36%)
  matrix products  122 us (36%)
  starting transfers between devices  35.8 us (10%)
  local copies, waits for them, and re-layouts  20.2 us (6%)
  other arithmetic  19.7 us (6%)
  between operations  13.8 us (4%)
  blocking collectives  5.27 us (2%)
    dot_general x16, matrix products, one_block(): jnp.einsum('cts,cs->ct', jnp.exp(gap), block_drive, precision=lax.Precisi...  111 us
    all_to_all x1, waiting for transfers between devices, per_device(): lax.all_to_all(outgoing, SP, split_axis=0, concat_axis=1, tiled=True)  55.7 us
    all_to_all x1, waiting for transfers between devices, moved_by_axis(): lax.all_to_all(tiles, axes[k], split_axis=k, concat_axis=k, tiled=True)  46.6 us
    all_to_all x1, starting transfers between devices, sent_to_all(): lax.all_to_all(jnp.broadcast_to(array[None], (count, *array.shape)), axis...  14.5 us
    all_to_all x1, waiting for transfers between devices, sent_to_all(): lax.all_to_all(jnp.broadcast_to(array[None], (count, *array.shape)), axis...  11.8 us
    all_to_all x1, waiting for transfers between devices, per_device(): lax.all_to_all(branch_out, 'tp', split_axis=1, concat_axis=0, tiled=True)  7.62 us
    all_to_all x1, starting transfers between devices, per_device(): lax.all_to_all(branch_out, 'tp', split_axis=1, concat_axis=0, tiled=True)  6.9 us
  transfers between devices with their start and end apart: 7, of which 4 were waited for; matrix products, arithmetic and copies ran while one was open for 43% of the time, Pallas kernels for 0%

commit v1 on v0

v1 whole, which is shorter than its diff:
```python
import functools
import math

import jax
import jax.numpy as jnp
from jax import lax
from jax.experimental import pallas as pl
from jax.experimental.pallas import tpu as pltpu
from jax.sharding import PartitionSpec as P

MESH = pl.DeviceIdType.MESH
F32 = jnp.float32
BF16 = jnp.bfloat16

epsilon = 1e-06
gate_power = 8.0
LANES = 128
COLS = 512
GROUP = 4


def one_minus_exp(y):
    series = F32(1.0 / 362880)
    for k in (40320, 5040, 720, 120, 24, 6, 2, 1):
        series = series * y + F32(1.0 / k)
    return jnp.where(y > -0.5, -y * series, 1.0 - jnp.exp(y))


def softplus(x):
    u = jnp.exp(-jnp.abs(x))
    series = F32(1.0 / 11)
    for k in range(10, 0, -1):
        series = F32(1.0 / k) - series * u
    return jnp.maximum(x, 0.0) + jnp.where(u < 0.125, u * series, jnp.log(1.0 + u))


def gelu(x):
    inner = F32(math.sqrt(2.0 / math.pi)) * (x + F32(0.044715) * (x * x * x))
    return x * (0.5 * (1.0 + jnp.tanh(inner)))


def to_column(row, size):
    lanes = row.shape[1]
    here = lax.broadcasted_iota(jnp.int32, (size, lanes), 0)
    there = lax.broadcasted_iota(jnp.int32, (size, lanes), 1)
    return jnp.sum(jnp.where(here == there, row, 0.0), axis=1, keepdims=True)


def kernel(
    cfg,
    resid_hbm,
    branch_ref,
    gate_ref,
    taps_ref,
    rate_w_ref,
    input_w_ref,
    base_ref,
    extra_ref,
    outw_hbm,
    gmix_ref,
    gpre_ref,
    gpost_ref,
    ids_ref,
    rw_ref,
    gp_hbm,
    up_hbm,
    dp_hbm,
    out_ref,
    resid_ref,
    keep_ref,
    state_ref,
    last_keep,
    last_state,
    act_ref,
    halo_ref,
    sum_ref,
    sums_ref,
    bo_ref,
    tok_ref,
    w_ref,
    e_ref,
    after_ref,
    ffn_ref,
    pick_ref,
    o_ref,
    x_ref,
    hid_ref,
    y_ref,
    r_ref,
    moe_ref,
    loc_sem,
    send_sem,
    recv_sem,
):
    nsp, nx, ny = cfg
    ntp = nx * ny
    sp = lax.axis_index("sp")
    tp = lax.axis_index("tp")
    my_x, my_y = lax.rem(tp, nx), lax.div(tp, nx)
    core = lax.rem(sp, 2)
    chan, positions = branch_ref.shape
    blocks = positions // LANES
    toks, width = resid_hbm.shape
    cap = o_ref.shape[1]
    slots = nsp * cap
    col_steps = width // COLS

    def remote(src, dst, k, to_sp, to_tp):
        return pltpu.make_async_remote_copy(
            src_ref=src, dst_ref=dst, send_sem=send_sem.at[k], recv_sem=recv_sem.at[k],
            device_id=(to_sp, to_tp), device_id_type=MESH,
        )

    def got(ref, k):
        pltpu.make_async_copy(ref, ref, recv_sem.at[k]).wait()

    def sent(ref, k):
        pltpu.make_async_copy(ref, ref, send_sem.at[k]).wait()

    own = [
        pltpu.make_async_copy(outw_hbm, w_ref.at[my_y, my_x], loc_sem.at[0]),
        pltpu.make_async_copy(gp_hbm, e_ref.at[0, my_y, my_x], loc_sem.at[1]),
        pltpu.make_async_copy(up_hbm, e_ref.at[1, my_y, my_x], loc_sem.at[2]),
        pltpu.make_async_copy(dp_hbm, e_ref.at[2, my_y, my_x], loc_sem.at[3]),
        pltpu.make_async_copy(resid_hbm, resid_ref, loc_sem.at[4]),
    ]
    for copy in own:
        copy.start()

    barrier = pltpu.get_barrier_semaphore()

    def greet_sp(k, carry):
        pl.semaphore_signal(
            barrier, inc=1, device_id=(lax.rem(sp + k, nsp), tp), device_id_type=MESH
        )
        return carry

    def greet_tp(k, carry):
        pl.semaphore_signal(
            barrier, inc=1, device_id=(sp, lax.rem(tp + k, ntp)), device_id_type=MESH
        )
        return carry

    lax.fori_loop(1, nsp, greet_sp, 0)
    lax.fori_loop(1, ntp, greet_tp, 0)

    taps = taps_ref[...].astype(F32)
    tap_cols = [to_column(taps[j : j + 1, :], chan) for j in range(4)]
    decay_rate = -gate_power * softplus(-to_column(base_ref[...], chan))
    lane = lax.broadcasted_iota(jnp.int32, (chan, LANES), 1)

    def lanes_of(index):
        return pl.ds(pl.multiple_of(index * LANES, LANES), LANES)

    def block_group(first, count, before):
        convs = []
        for g in range(count):
            cur = branch_ref[:, lanes_of(first + g)].astype(F32)
            total = tap_cols[3] * cur
            for back in (1, 2, 3):
                moved = jnp.where(
                    lane < back, pltpu.roll(before, back, 1), pltpu.roll(cur, back, 1)
                )
                total = total + tap_cols[3 - back] * moved
            convs.append(total)
            before = cur
        conv = jnp.concatenate(convs, axis=1)
        high = conv.astype(BF16)
        rest = conv - high.astype(F32)
        mid = rest.astype(BF16)
        low = (rest - mid.astype(F32)).astype(BF16)

        def gate_of(weight_ref):
            w = weight_ref[...]
            total = None
            for piece in (low, mid, high):
                part = lax.dot_general(
                    w, piece, (((0,), (0,)), ((), ())), preferred_element_type=F32
                )
                total = part if total is None else total + part
            return jax.nn.sigmoid(total)

        rate_gate = gate_of(rate_w_ref)
        input_gate = gate_of(input_w_ref)
        for g in range(count):
            at = slice(g * LANES, (g + 1) * LANES)
            extra = extra_ref[pl.ds(first + g, 1), :]
            log_keep = decay_rate * rate_gate[:, at] + extra
            keep = jnp.exp(log_keep)
            state = jnp.sqrt(one_minus_exp(2.0 * log_keep)) * input_gate[:, at] * convs[g]
            step = 1
            while step < LANES:
                inside = lane >= step
                keep_back = jnp.where(inside, pltpu.roll(keep, step, 1), 1.0)
                state_back = jnp.where(inside, pltpu.roll(state, step, 1), 0.0)
                state = keep * state_back + state
                keep = keep * keep_back
                step *= 2
            keep_ref[first + g] = keep
            state_ref[first + g] = state
            last_keep[first + g] = jnp.broadcast_to(keep[:, LANES - 1 :], (chan, LANES))
            last_state[first + g] = jnp.broadcast_to(state[:, LANES - 1 :], (chan, LANES))

    group = min(GROUP, blocks)

    def later_group(index, carry):
        first = index * group
        block_group(first, group, branch_ref[:, lanes_of(first - 1)].astype(F32))
        return carry

    lax.fori_loop(1, blocks // group, later_group, 0)

    pl.semaphore_wait(barrier, nsp - 1 + ntp - 1)
    remote(
        branch_ref.at[:, pl.ds(positions - LANES, LANES)], halo_ref, 0, lax.rem(sp + 1, nsp), tp
    ).start()

    own[0].wait()
    half_a, half_b = 2 * core, 2 * core + 1

    def tp_at(y, x):
        return lax.rem(y, ny) * nx + lax.rem(x, nx)

    for k in range(1, nx):
        ref = w_ref.at[my_y, my_x, half_a]
        remote(ref, ref, 1, sp, tp_at(my_y, my_x + k)).start()
    for k in range(1, ny):
        ref = w_ref.at[my_y, my_x, half_b]
        remote(ref, ref, 2, sp, tp_at(my_y + k, my_x)).start()

    got(halo_ref, 0)
    block_group(0, group, jnp.where(sp == 0, 0.0, halo_ref[...].astype(F32)))

    def chain(index, carry):
        keep, state = carry
        block_keep, block_state = last_keep[index], last_state[index]
        last_keep[index] = keep
        last_state[index] = state
        return (block_keep * keep, block_keep * state + block_state)

    all_keep, all_state = lax.fori_loop(
        0, blocks, chain, (jnp.ones((chan, LANES), F32), jnp.zeros((chan, LANES), F32))
    )
    row = lax.broadcasted_iota(jnp.int32, (chan, LANES), 0)
    summary = jnp.where(lane == row, all_keep, 0.0) + jnp.where(
        lane == row + chan, all_state, 0.0
    )
    sum_ref[...] = jnp.sum(summary, axis=0, keepdims=True)
    sums_ref[sp] = sum_ref[...]

    got(w_ref.at[0, pl.ds(0, nx - 1), 0], 1)
    for k in range(1, ny):
        ref = w_ref.at[my_y, :, half_a]
        remote(ref, ref, 3, sp, tp_at(my_y + k, my_x)).start()
    got(w_ref.at[pl.ds(0, ny - 1), 0, 0], 2)
    for k in range(1, nx):
        ref = w_ref.at[:, my_x, half_b]
        remote(ref, ref, 4, sp, tp_at(my_y, my_x + k)).start()

    def send_summary(k, carry):
        remote(sum_ref, sums_ref.at[sp], 5, lax.rem(sp + k, nsp), tp).start()
        return carry

    lax.fori_loop(1, nsp, send_summary, 0)

    def activate(index, carry):
        act_ref[index] = gelu(gate_ref[:, lanes_of(index)].astype(F32))
        return carry

    lax.fori_loop(0, blocks, activate, 0)

    ids = ids_ref[...]
    expert = lax.broadcasted_iota(jnp.int32, (nsp, toks), 0)
    named = [expert == ids[k : k + 1, :] for k in range(2)]
    counts = (named[0] | named[1]).astype(F32)
    token_a = lax.broadcasted_iota(jnp.int32, (toks, toks), 0)
    token_b = lax.broadcasted_iota(jnp.int32, (toks, toks), 1)
    earlier = jnp.dot(
        counts.astype(BF16), (token_a < token_b).astype(F32).astype(BF16),
        preferred_element_type=F32,
    )
    slot_at = [
        jnp.sum(
            jnp.where(named[k], earlier + (expert * cap).astype(F32), 0.0), axis=0, keepdims=True
        ).astype(jnp.int32)
        for k in range(2)
    ]
    slot = lax.broadcasted_iota(jnp.int32, (slots, toks), 0)
    chosen = [slot == slot_at[k] for k in range(2)]
    pick_ref[0] = (chosen[0] | chosen[1]).astype(F32).astype(BF16)
    weight = jnp.where(chosen[0], rw_ref[0:1, :], 0.0) + jnp.where(chosen[1], rw_ref[1:2, :], 0.0)
    weight_high = weight.astype(BF16)
    pick_ref[1] = weight_high
    pick_ref[2] = (weight - weight_high.astype(F32)).astype(BF16)

    got(sums_ref.at[pl.ds(0, nsp - 1)], 5)

    def fold(index, carry):
        line = sums_ref[index]
        keep = jnp.where(index < sp, to_column(line, chan), 1.0)
        moved = jnp.where(
            index < sp,
            jnp.sum(jnp.where(lane == row + chan, line, 0.0), axis=1, keepdims=True),
            0.0,
        )
        return keep * carry + moved

    entering = lax.fori_loop(0, nsp, fold, jnp.zeros((chan, 1), F32), unroll=True)

    def finish(index, carry):
        begin = last_state[index] + last_keep[index] * entering
        hidden = state_ref[index] + keep_ref[index] * begin
        bo_ref[index] = (hidden * act_ref[index]).astype(BF16)
        return carry

    lax.fori_loop(0, blocks, finish, 0)

    def send_tokens(k, carry):
        to = lax.rem(tp + k, ntp)
        remote(bo_ref.at[to], tok_ref.at[tp], 6, sp, to).start()
        return carry

    lax.fori_loop(1, ntp, send_tokens, 0)
    tok_ref[tp] = bo_ref[tp]

    got(w_ref.at[pl.ds(0, ny - 1), :, 0], 3)
    got(w_ref.at[:, pl.ds(0, nx - 1), 0], 4)
    ref = w_ref.at[:, :, pl.ds(2 * core, 2)]
    remote(ref, ref, 7, sp + 1 - 2 * core, tp).start()

    for copy in own[1:4]:
        copy.wait()
    for k in range(1, nx):
        ref = e_ref.at[:, my_y, my_x, 0]
        remote(ref, ref, 8, sp, tp_at(my_y, my_x + k)).start()
    for k in range(1, ny):
        ref = e_ref.at[:, my_y, my_x, 1]
        remote(ref, ref, 9, sp, tp_at(my_y + k, my_x)).start()

    own[4].wait()
    got(tok_ref.at[pl.ds(0, ntp - 1)], 6)
    got(w_ref.at[:, :, pl.ds(0, 2)], 7)

    def cols_of(index):
        return pl.ds(pl.multiple_of(index * COLS, COLS), COLS)

    def mix(index, carry):
        cols = cols_of(index)
        weights = w_ref[:, :, :, :, cols].reshape(ntp * chan, COLS)
        rows = tok_ref[...].reshape(ntp * chan, toks)
        after_ref[:, cols] = lax.dot_general(
            rows, weights, (((0,), (0,)), ((), ())), preferred_element_type=F32
        )
        return carry

    lax.fori_loop(0, col_steps, mix, 0)

    def scale(values):
        return lax.rsqrt(jnp.mean(values * values, axis=-1, keepdims=True) + epsilon)

    def rows_of(index):
        return pl.ds(pl.multiple_of(index * 16, 16), 16)

    def norms(index, carry):
        rows = rows_of(index)
        mixed = after_ref[rows, :]
        after = resid_ref[rows, :].astype(F32) + mixed * scale(mixed) * gmix_ref[...]
        after_ref[rows, :] = after
        ffn_ref[rows, :] = (after * scale(after) * gpre_ref[...]).astype(BF16)
        return carry

    lax.fori_loop(0, toks // 16, norms, 0)

    def spread(index, carry):
        cols = cols_of(index)
        o_ref[:, :, cols] = (
            jnp.dot(pick_ref[0], ffn_ref[:, cols], preferred_element_type=F32)
            .astype(BF16)
            .reshape(nsp, cap, COLS)
        )
        return carry

    lax.fori_loop(0, col_steps, spread, 0)

    def peer(k):
        away = lax.div(k + 1, 2)
        return lax.rem(lax.rem(k, 2) * away + (1 - lax.rem(k, 2)) * (nsp - away) + sp, nsp)

    def dispatch(k, carry):
        to = peer(k)
        remote(o_ref.at[to], x_ref.at[sp], 10, to, tp).start()
        return carry

    lax.fori_loop(1, nsp, dispatch, 0)
    x_ref[sp] = o_ref[sp]

    got(e_ref.at[:, 0, pl.ds(0, nx - 1), 0], 8)
    for k in range(1, ny):
        ref = e_ref.at[:, my_y, :, 0]
        remote(ref, ref, 11, sp, tp_at(my_y + k, my_x)).start()
    got(e_ref.at[:, pl.ds(0, ny - 1), 0, 1], 9)
    for k in range(1, nx):
        ref = e_ref.at[:, :, my_x, 1]
        remote(ref, ref, 12, sp, tp_at(my_y, my_x + k)).start()

    got(e_ref.at[:, pl.ds(0, ny - 1), :, 0], 11)
    got(e_ref.at[:, :, pl.ds(0, nx - 1), 1], 12)
    got(x_ref.at[pl.ds(0, nsp - 1)], 10)

    per_y = nx * 32
    nt = (((1,), (1,)), ((), ()))

    def expert_in(index, carry):
        ys = pl.ds(index * 2, 2)
        arriving = x_ref[...].reshape(slots, width)
        gate_rows = e_ref[0, ys].reshape(2 * per_y, width)
        up_rows = e_ref[1, ys].reshape(2 * per_y, width)
        gate_vals = lax.dot_general(arriving, gate_rows, nt, preferred_element_type=F32)
        up_vals = lax.dot_general(arriving, up_rows, nt, preferred_element_type=F32)
        hid_ref[index] = (gate_vals * jax.nn.sigmoid(gate_vals) * up_vals).astype(BF16)
        return carry

    lax.fori_loop(0, ny // 2, expert_in, 0)

    def expert_out(index, carry):
        cols = cols_of(index)
        total = None
        for half in range(ny // 2):
            down = e_ref[2, 2 * half : 2 * half + 2, :, :, :, cols].reshape(2 * per_y, COLS)
            part = jnp.dot(hid_ref[half], down, preferred_element_type=F32)
            total = part if total is None else total + part
        y_ref[:, :, cols] = total.astype(BF16).reshape(nsp, cap, COLS)
        return carry

    lax.fori_loop(0, col_steps, expert_out, 0)

    def give_back(k, carry):
        to = peer(k)
        remote(y_ref.at[to], r_ref.at[sp], 13, to, tp).start()
        return carry

    lax.fori_loop(1, nsp, give_back, 0)
    r_ref[sp] = y_ref[sp]
    got(r_ref.at[pl.ds(0, nsp - 1)], 13)

    def combine(index, carry):
        cols = cols_of(index)
        rows = r_ref[:, :, cols].reshape(slots, COLS)
        tn = (((0,), (0,)), ((), ()))
        moe_ref[:, cols] = lax.dot_general(
            pick_ref[2], rows, tn, preferred_element_type=F32
        ) + lax.dot_general(pick_ref[1], rows, tn, preferred_element_type=F32)
        return carry

    lax.fori_loop(0, col_steps, combine, 0)

    def finalize(index, carry):
        rows = rows_of(index)
        moe = moe_ref[rows, :]
        out_ref[rows, :] = (after_ref[rows, :] + moe * scale(moe) * gpost_ref[...]).astype(BF16)
        return carry

    lax.fori_loop(0, toks // 16, finalize, 0)

    sent(halo_ref, 0)
    sent(w_ref.at[0, pl.ds(0, nx - 1), 0], 1)
    sent(w_ref.at[pl.ds(0, ny - 1), 0, 0], 2)
    sent(w_ref.at[pl.ds(0, ny - 1), :, 0], 3)
    sent(w_ref.at[:, pl.ds(0, nx - 1), 0], 4)
    sent(sums_ref.at[pl.ds(0, nsp - 1)], 5)
    sent(tok_ref.at[pl.ds(0, ntp - 1)], 6)
    sent(w_ref.at[:, :, pl.ds(0, 2)], 7)
    sent(e_ref.at[:, 0, pl.ds(0, nx - 1), 0], 8)
    sent(e_ref.at[:, pl.ds(0, ny - 1), 0, 1], 9)
    sent(x_ref.at[pl.ds(0, nsp - 1)], 10)
    sent(e_ref.at[:, pl.ds(0, ny - 1), :, 0], 11)
    sent(e_ref.at[:, :, pl.ds(0, nx - 1), 1], 12)
    sent(r_ref.at[pl.ds(0, nsp - 1)], 13)


def solution(mesh):
    nsp, ntp = mesh.shape["sp"], mesh.shape["tp"]
    nx = math.isqrt(ntp)
    ny = ntp // nx

    def per_device(
        resid, branch_input, gate_in, conv_taps, rate_weight, input_weight, decay_base,
        decay_extra, out_weight, gain_mix, gain_pre, gain_post, expert_ids, route_weight,
        gate_proj, up_proj, down_proj,
    ):
        chan, positions = branch_input.shape
        toks, width = resid.shape
        blocks = positions // LANES
        cap = 2 * toks // nsp
        vmem = pl.BlockSpec(memory_space=pltpu.VMEM)
        hbm = pl.BlockSpec(memory_space=pl.ANY)
        block = (blocks, chan, LANES)
        return pl.pallas_call(
            functools.partial(kernel, (nsp, nx, ny)),
            out_shape=jax.ShapeDtypeStruct((toks, width), BF16),
            in_specs=[hbm] + [vmem] * 7 + [hbm] + [vmem] * 5 + [hbm] * 3,
            out_specs=vmem,
            scratch_shapes=[
                pltpu.VMEM((toks, width), BF16),
                pltpu.VMEM(block, F32),
                pltpu.VMEM(block, F32),
                pltpu.VMEM(block, F32),
                pltpu.VMEM(block, F32),
                pltpu.VMEM(block, F32),
                pltpu.VMEM((chan, LANES), BF16),
                pltpu.VMEM((1, LANES), F32),
                pltpu.VMEM((nsp, 1, LANES), F32),
                pltpu.VMEM(block, BF16),
                pltpu.VMEM((ntp, chan, toks), BF16),
                pltpu.VMEM((ny, nx, 4, chan // 4, width), BF16),
                pltpu.VMEM((3, ny, nx, 2, 16, width), BF16),
                pltpu.VMEM((toks, width), F32),
                pltpu.VMEM((toks, width), BF16),
                pltpu.VMEM((3, nsp * cap, toks), BF16),
                pltpu.VMEM((nsp, cap, width), BF16),
                pltpu.VMEM((nsp, cap, width), BF16),
                pltpu.VMEM((ny // 2, nsp * cap, nx * 64), BF16),
                pltpu.VMEM((nsp, cap, width), BF16),
                pltpu.VMEM((nsp, cap, width), BF16),
                pltpu.VMEM((toks, width), F32),
                pltpu.SemaphoreType.DMA((5,)),
                pltpu.SemaphoreType.DMA((14,)),
                pltpu.SemaphoreType.DMA((14,)),
            ],
            compiler_params=pltpu.CompilerParams(
                collective_id=0, has_side_effects=True, vmem_limit_bytes=52 * 1024 * 1024
            ),
        )(
            resid, branch_input, gate_in, conv_taps,
            rate_weight.reshape(chan, chan), input_weight.reshape(chan, chan),
            decay_base.reshape(1, chan), decay_extra.reshape(blocks, LANES),
            out_weight.reshape(4, chan // 4, width),
            gain_mix.reshape(1, width), gain_pre.reshape(1, width), gain_post.reshape(1, width),
            expert_ids.T, route_weight.T,
            gate_proj.reshape(2, 16, width), up_proj.reshape(2, 16, width),
            down_proj.reshape(2, 16, width),
        )

    sp_tp = P(("sp", "tp"), None)
    experts = P("sp", "tp", None)
    return jax.shard_map(
        per_device,
        mesh=mesh,
        in_specs=(
            sp_tp, P("tp", "sp"), P("tp", "sp"), P(None, "tp"),
            P("tp", None, None), P("tp", None, None), P("tp"), P("sp"), P("tp", None),
            P(), P(), P(), sp_tp, sp_tp, experts, experts, experts,
        ),
        out_specs=sp_tp,
        check_vma=False,
    )
```

time: 343 us -> 163 us (0.48)
  the two profiles are of different devices: /device:TPU:1 before, /device:TPU:36 now
where the time goes in v1:
time: 163 us
  Pallas kernels  151 us (93%)
  local copies, waits for them, and re-layouts  11.9 us (7%)
    pallas_call x1, Pallas kernels, per_device(): pl.pallas_call(functools.partial(kernel, (nsp, nx, ny)), out_shape=jax.Sh...  151 us
    unnamed x33, local copies, waits for them, and re-layouts  11.9 us

profile of v1, /device:TPU:36, one launch (start us, length us, event | category | flops | bytes accessed | tf_op | source)
XLA Modules:
  0.0 162.5 jit_solution(5230492768874050140)
XLA Ops:
  0.0 0.0 copy-start.6
  0.0 0.0 copy-start.8
  0.0 0.0 copy-start.15
  0.0 0.7 copy-done.6
  0.7 0.0 copy-done.8
  0.7 0.0 copy-done.15
  0.7 0.0 copy-start
  0.7 0.9 copy-done
  1.7 0.0 copy-start.1
  1.7 0.9 copy-done.1
  2.6 0.0 copy-start.2
  2.6 0.9 copy-done.2
  3.6 0.0 copy-start.3
  3.6 0.9 copy-done.3
  4.5 0.0 copy-start.4
  4.5 0.9 copy-done.4
  5.4 0.0 copy-start.5
  5.4 0.9 copy-done.5
  6.3 0.0 copy-start.7
  6.3 0.7 copy-done.7
  7.0 0.0 copy-start.9
  7.0 0.7 copy-done.9
  7.7 0.0 copy-start.10
  7.7 0.7 copy-done.10
  8.4 0.0 copy-start.11
  8.4 0.7 copy-done.11
  9.1 0.0 copy-start.12
  9.1 0.7 copy-done.12
  9.8 0.0 copy-start.13
  9.8 0.7 copy-done.13
  10.5 0.0 copy-start.14
  10.5 0.7 copy-done.14
  11.1 150.6 %shard_map.163 = bf16[128,2048]{1,0:T(8,128)(2,1)S(1)} custom-call(bf16[128,2048]{1,0:T(8,128)(2,1)} %resid_hbm.1, bf16[64,2048]{1,0:T(8,128)(2,1)S(1)} %copy-done, bf16[64,2048]{1,0:T(8,128)(2,1)S(1)} %copy-done.1, bf16[4,64]{1,0:T(4,128)(2,1)S(1)} %copy-done.12, bf16[64,64]{1,0:T(8,128)(2,1)S(1)} %bitcast.17, bf16[64,64]{1,0:T(8,128)(2,1)S(1)} %bitcast.18, ...), custom_call_target="tpu_custom_call" | custom-call | tf_op jit(solution)/shard_map/pallas_call | solution.py:498
  161.7 0.8 copy.19
Async XLA Ops:
  0.0 0.7 copy-start.6
  0.0 0.7 copy-start.8
  0.0 0.7 copy-start.15
  0.7 1.0 copy-start
  1.7 0.9 copy-start.1
  2.6 0.9 copy-start.2
  3.6 0.9 copy-start.3
  4.5 0.9 copy-start.4
  5.4 0.9 copy-start.5
  6.3 0.7 copy-start.7
  7.0 0.7 copy-start.9
  7.7 0.7 copy-start.10
  8.4 0.7 copy-start.11
  9.1 0.7 copy-start.12
  9.8 0.7 copy-start.13
  10.5 0.7 copy-start.14

commit v2 on v1

--- a/solution.py
+++ b/solution.py
@@ -17,6 +17,7 @@
 LANES = 128
 COLS = 512
 GROUP = 4
+FAR = 22
 
 
 def one_minus_exp(y):
@@ -49,19 +50,19 @@
 def kernel(
     cfg,
     resid_hbm,
-    branch_ref,
-    gate_ref,
-    taps_ref,
-    rate_w_ref,
-    input_w_ref,
-    base_ref,
-    extra_ref,
+    branch_hbm,
+    gate_hbm,
+    taps_hbm,
+    rate_w_hbm,
+    input_w_hbm,
+    base_hbm,
+    extra_hbm,
     outw_hbm,
-    gmix_ref,
-    gpre_ref,
-    gpost_ref,
-    ids_ref,
-    rw_ref,
+    gmix_hbm,
+    gpre_hbm,
+    gpost_hbm,
+    ids_hbm,
+    rw_hbm,
     gp_hbm,
     up_hbm,
     dp_hbm,
@@ -84,10 +85,27 @@
     pick_ref,
     o_ref,
     x_ref,
+    on_ref,
+    ob_ref,
+    xb_ref,
+    m_ref,
+    xf_ref,
     hid_ref,
     y_ref,
     r_ref,
     moe_ref,
+    branch_ref,
+    gate_ref,
+    taps_ref,
+    rate_w_ref,
+    input_w_ref,
+    base_ref,
+    extra_ref,
+    gmix_ref,
+    gpre_ref,
+    gpost_ref,
+    ids_ref,
+    rw_ref,
     loc_sem,
     send_sem,
     recv_sem,
@@ -98,7 +116,7 @@
     tp = lax.axis_index("tp")
     my_x, my_y = lax.rem(tp, nx), lax.div(tp, nx)
     core = lax.rem(sp, 2)
-    chan, positions = branch_ref.shape
+    chan, positions = branch_hbm.shape
     blocks = positions // LANES
     toks, width = resid_hbm.shape
     cap = o_ref.shape[1]
@@ -124,7 +142,16 @@
         pltpu.make_async_copy(dp_hbm, e_ref.at[2, my_y, my_x], loc_sem.at[3]),
         pltpu.make_async_copy(resid_hbm, resid_ref, loc_sem.at[4]),
     ]
-    for copy in own:
+    small = [
+        pltpu.make_async_copy(source, target, loc_sem.at[5 + k])
+        for k, (source, target) in enumerate((
+            (branch_hbm, branch_ref), (taps_hbm, taps_ref), (rate_w_hbm, rate_w_ref),
+            (input_w_hbm, input_w_ref), (base_hbm, base_ref), (extra_hbm, extra_ref),
+            (gate_hbm, gate_ref), (ids_hbm, ids_ref), (rw_hbm, rw_ref),
+            (gmix_hbm, gmix_ref), (gpre_hbm, gpre_ref), (gpost_hbm, gpost_ref),
+        ))
+    ]
+    for copy in small + own:
         copy.start()
 
     barrier = pltpu.get_barrier_semaphore()
@@ -143,6 +170,9 @@
 
     lax.fori_loop(1, nsp, greet_sp, 0)
     lax.fori_loop(1, ntp, greet_tp, 0)
+
+    for copy in small[:6]:
+        copy.wait()
 
     taps = taps_ref[...].astype(F32)
     tap_cols = [to_column(taps[j : j + 1, :], chan) for j in range(4)]
@@ -210,58 +240,8 @@
 
     lax.fori_loop(1, blocks // group, later_group, 0)
 
-    pl.semaphore_wait(barrier, nsp - 1 + ntp - 1)
-    remote(
-        branch_ref.at[:, pl.ds(positions - LANES, LANES)], halo_ref, 0, lax.rem(sp + 1, nsp), tp
-    ).start()
-
-    own[0].wait()
-    half_a, half_b = 2 * core, 2 * core + 1
-
-    def tp_at(y, x):
-        return lax.rem(y, ny) * nx + lax.rem(x, nx)
-
-    for k in range(1, nx):
-        ref = w_ref.at[my_y, my_x, half_a]
-        remote(ref, ref, 1, sp, tp_at(my_y, my_x + k)).start()
-    for k in range(1, ny):
-        ref = w_ref.at[my_y, my_x, half_b]
-        remote(ref, ref, 2, sp, tp_at(my_y + k, my_x)).start()
-
-    got(halo_ref, 0)
-    block_group(0, group, jnp.where(sp == 0, 0.0, halo_ref[...].astype(F32)))
-
-    def chain(index, carry):
-        keep, state = carry
-        block_keep, block_state = last_keep[index], last_state[index]
-        last_keep[index] = keep
-        last_state[index] = state
-        return (block_keep * keep, block_keep * state + block_state)
-
-    all_keep, all_state = lax.fori_loop(
-        0, blocks, chain, (jnp.ones((chan, LANES), F32), jnp.zeros((chan, LANES), F32))
-    )
-    row = lax.broadcasted_iota(jnp.int32, (chan, LANES), 0)
-    summary = jnp.where(lane == row, all_keep, 0.0) + jnp.where(
-        lane == row + chan, all_state, 0.0
-    )
-    sum_ref[...] = jnp.sum(summary, axis=0, keepdims=True)
-    sums_ref[sp] = sum_ref[...]
-
-    got(w_ref.at[0, pl.ds(0, nx - 1), 0], 1)
-    for k in range(1, ny):
-        ref = w_ref.at[my_y, :, half_a]
-        remote(ref, ref, 3, sp, tp_at(my_y + k, my_x)).start()
-    got(w_ref.at[pl.ds(0, ny - 1), 0, 0], 2)
-    for k in range(1, nx):
-        ref = w_ref.at[:, my_x, half_b]
-        remote(ref, ref, 4, sp, tp_at(my_y, my_x + k)).start()
-
-    def send_summary(k, carry):
-        remote(sum_ref, sums_ref.at[sp], 5, lax.rem(sp + k, nsp), tp).start()
-        return carry
-
-    lax.fori_loop(1, nsp, send_summary, 0)
+    for copy in small[6:]:
+        copy.wait()
 
     def activate(index, carry):
         act_ref[index] = gelu(gate_ref[:, lanes_of(index)].astype(F32))
@@ -293,40 +273,64 @@
     pick_ref[1] = weight_high
     pick_ref[2] = (weight - weight_high.astype(F32)).astype(BF16)
 
-    got(sums_ref.at[pl.ds(0, nsp - 1)], 5)
-
-    def fold(index, carry):
-        line = sums_ref[index]
-        keep = jnp.where(index < sp, to_column(line, chan), 1.0)
-        moved = jnp.where(
-            index < sp,
-            jnp.sum(jnp.where(lane == row + chan, line, 0.0), axis=1, keepdims=True),
-            0.0,
-        )
-        return keep * carry + moved
-
-    entering = lax.fori_loop(0, nsp, fold, jnp.zeros((chan, 1), F32), unroll=True)
-
-    def finish(index, carry):
-        begin = last_state[index] + last_keep[index] * entering
-        hidden = state_ref[index] + keep_ref[index] * begin
-        bo_ref[index] = (hidden * act_ref[index]).astype(BF16)
-        return carry
-
-    lax.fori_loop(0, blocks, finish, 0)
-
-    def send_tokens(k, carry):
-        to = lax.rem(tp + k, ntp)
-        remote(bo_ref.at[to], tok_ref.at[tp], 6, sp, to).start()
-        return carry
-
-    lax.fori_loop(1, ntp, send_tokens, 0)
-    tok_ref[tp] = bo_ref[tp]
-
-    got(w_ref.at[pl.ds(0, ny - 1), :, 0], 3)
-    got(w_ref.at[:, pl.ds(0, nx - 1), 0], 4)
-    ref = w_ref.at[:, :, pl.ds(2 * core, 2)]
-    remote(ref, ref, 7, sp + 1 - 2 * core, tp).start()
+    own[4].wait()
+
+    def cols_of(index):
+        return pl.ds(pl.multiple_of(index * COLS, COLS), COLS)
+
+    def spread(rows_ref, slots_ref):
+        def some(index, carry):
+            cols = cols_of(index)
+            slots_ref[:, :, cols] = (
+                jnp.dot(pick_ref[0], rows_ref[:, cols], preferred_element_type=F32)
+                .astype(BF16)
+                .reshape(nsp, cap, COLS)
+            )
+            return carry
+
+        lax.fori_loop(0, col_steps, some, 0)
+
+    spread(resid_ref, o_ref)
+
+    far = nsp * FAR // 32
+
+    def peer(k):
+        away = lax.div(k + 1, 2)
+        return lax.rem(lax.rem(k, 2) * away + (1 - lax.rem(k, 2)) * (nsp - away) + sp, nsp)
+
+    def send_block(source, target, sem, k, place):
+        to = peer(k)
+        remote(source.at[to], target.at[place], sem, to, tp).start()
+
+    def send_blocks(source, target, sem, begin, end, offset=0):
+        def step(k, carry):
+            send_block(source, target, sem, k, k + 2 * lax.rem(k, 2) - 1 - offset)
+            return carry
+
+        lax.fori_loop(begin, end, step, 0)
+
+    first_batch = min(far + 2, nsp - 1)
+
+    pl.semaphore_wait(barrier, nsp - 1 + ntp - 1)
+    remote(
+        branch_ref.at[:, pl.ds(positions - LANES, LANES)], halo_ref, 0, lax.rem(sp + 1, nsp), tp
+    ).start()
+
+    send_block(o_ref, x_ref, 14, far - 1, far)
+    send_blocks(o_ref, x_ref, 14, far + 1, first_batch)
+
+    own[0].wait()
+    half_a, half_b = 2 * core, 2 * core + 1
+
+    def tp_at(y, x):
+        return lax.rem(y, ny) * nx + lax.rem(x, nx)
+
+    for k in range(1, nx):
+        ref = w_ref.at[my_y, my_x, half_a]
+        remote(ref, ref, 1, sp, tp_at(my_y, my_x + k)).start()
+    for k in range(1, ny):
+        ref = w_ref.at[my_y, my_x, half_b]
+        remote(ref, ref, 2, sp, tp_at(my_y + k, my_x)).start()
 
     for copy in own[1:4]:
         copy.wait()
@@ -337,33 +341,123 @@
         ref = e_ref.at[:, my_y, my_x, 1]
         remote(ref, ref, 9, sp, tp_at(my_y + k, my_x)).start()
 
-    own[4].wait()
+    got(halo_ref, 0)
+    block_group(0, group, jnp.where(sp == 0, 0.0, halo_ref[...].astype(F32)))
+
+    def chain(index, carry):
+        keep, state = carry
+        block_keep, block_state = last_keep[index], last_state[index]
+        last_keep[index] = keep
+        last_state[index] = state
+        return (block_keep * keep, block_keep * state + block_state)
+
+    all_keep, all_state = lax.fori_loop(
+        0, blocks, chain, (jnp.ones((chan, LANES), F32), jnp.zeros((chan, LANES), F32))
+    )
+    row = lax.broadcasted_iota(jnp.int32, (chan, LANES), 0)
+    summary = jnp.where(lane == row, all_keep, 0.0) + jnp.where(
+        lane == row + chan, all_state, 0.0
+    )
+    sum_ref[...] = jnp.sum(summary, axis=0, keepdims=True)
+    sums_ref[sp] = sum_ref[...]
+
+    def send_summary(k, carry):
+        remote(sum_ref, sums_ref.at[sp], 5, lax.rem(sp + k, nsp), tp).start()
+        return carry
+
+    lax.fori_loop(1, nsp, send_summary, 0)
+    send_blocks(o_ref, x_ref, 14, first_batch, nsp - 1)
+    send_block(o_ref, x_ref, 14, nsp - 1, nsp - 1)
+
+    got(sums_ref.at[pl.ds(0, nsp - 1)], 5)
+
+    def fold(index, carry):
+        line = sums_ref[index]
+        keep = jnp.where(index < sp, to_column(line, chan), 1.0)
+        moved = jnp.where(
+            index < sp,
+            jnp.sum(jnp.where(lane == row + chan, line, 0.0), axis=1, keepdims=True),
+            0.0,
+        )
+        return keep * carry + moved
+
+    entering = lax.fori_loop(0, nsp, fold, jnp.zeros((chan, 1), F32), unroll=True)
+
+    def finish(index, carry):
+        begin = last_state[index] + last_keep[index] * entering
+        hidden = state_ref[index] + keep_ref[index] * begin
+        bo_ref[index] = (hidden * act_ref[index]).astype(BF16)
+        return carry
+
+    lax.fori_loop(0, blocks, finish, 0)
+
+    def send_tokens(k, carry):
+        to = lax.rem(tp + k, ntp)
+        remote(bo_ref.at[to], tok_ref.at[tp], 6, sp, to).start()
+        return carry
+
+    lax.fori_loop(1, ntp, send_tokens, 0)
+    tok_ref[tp] = bo_ref[tp]
+
+    got(w_ref.at[0, pl.ds(0, nx - 1), 0], 1)
+    for k in range(1, ny):
+        ref = w_ref.at[my_y, :, half_a]
+        remote(ref, ref, 3, sp, tp_at(my_y + k, my_x)).start()
+    got(w_ref.at[pl.ds(0, ny - 1), 0, 0], 2)
+    for k in range(1, nx):
+        ref = w_ref.at[:, my_x, half_b]
+        remote(ref, ref, 4, sp, tp_at(my_y, my_x + k)).start()
+
+    got(e_ref.at[:, 0, pl.ds(0, nx - 1), 0], 8)
+    for k in sorted({1, ny - 1}):
+        ref = e_ref.at[:, my_y, :, 0]
+        remote(ref, ref, 11, sp, tp_at(my_y + k, my_x)).start()
+    got(e_ref.at[:, pl.ds(0, ny - 1), 0, 1], 9)
+    for k in sorted({1, nx - 1}):
+        ref = e_ref.at[:, :, my_x, 1]
+        remote(ref, ref, 12, sp, tp_at(my_y, my_x + k)).start()
+
     got(tok_ref.at[pl.ds(0, ntp - 1)], 6)
+    ob_ref[...] = (
+        lax.dot_general(
+            pick_ref[0], tok_ref[...].reshape(ntp * chan, toks), (((1,), (1,)), ((), ())),
+            preferred_element_type=F32,
+        )
+        .astype(BF16)
+        .reshape(nsp, cap, ntp * chan)
+    )
+    send_block(ob_ref, xb_ref, 15, far - 1, 0)
+    send_blocks(ob_ref, xb_ref, 15, far + 1, nsp - 1, far)
+    send_block(ob_ref, xb_ref, 15, nsp - 1, nsp - 1 - far)
+
+    got(w_ref.at[pl.ds(0, ny - 1), :, 0], 3)
+    got(w_ref.at[:, pl.ds(0, nx - 1), 0], 4)
+    ref = w_ref.at[:, :, pl.ds(2 * core, 2)]
+    remote(ref, ref, 7, sp + 1 - 2 * core, tp).start()
     got(w_ref.at[:, :, pl.ds(0, 2)], 7)
 
-    def cols_of(index):
-        return pl.ds(pl.multiple_of(index * COLS, COLS), COLS)
+    def scale(values):
+        return lax.rsqrt(jnp.mean(values * values, axis=-1, keepdims=True) + epsilon)
+
+    def rows_of(index):
+        return pl.ds(pl.multiple_of(index * 16, 16), 16)
+
+    def projection(cols):
+        return w_ref[:, :, :, :, cols].reshape(ntp * chan, COLS)
 
     def mix(index, carry):
         cols = cols_of(index)
-        weights = w_ref[:, :, :, :, cols].reshape(ntp * chan, COLS)
         rows = tok_ref[...].reshape(ntp * chan, toks)
-        after_ref[:, cols] = lax.dot_general(
-            rows, weights, (((0,), (0,)), ((), ())), preferred_element_type=F32
+        moe_ref[:, cols] = lax.dot_general(
+            rows, projection(cols), (((0,), (0,)), ((), ())), preferred_element_type=F32
         )
         return carry
 
     lax.fori_loop(0, col_steps, mix, 0)
-
-    def scale(values):
-        return lax.rsqrt(jnp.mean(values * values, axis=-1, keepdims=True) + epsilon)
-
-    def rows_of(index):
-        return pl.ds(pl.multiple_of(index * 16, 16), 16)
 
     def norms(index, carry):
         rows = rows_of(index)
-        mixed = after_ref[rows, :]
+        mixed = moe_ref[rows, :]
         after = resid_ref[rows, :].astype(F32) + mixed * scale(mixed) * gmix_ref[...]
         after_ref[rows, :] = after
         ffn_ref[rows, :] = (after * scale(after) * gpre_ref[...]).astype(BF16)
@@ -371,76 +465,110 @@
 
     lax.fori_loop(0, toks // 16, norms, 0)
 
-    def spread(index, carry):
-        cols = cols_of(index)
-        o_ref[:, :, cols] = (
-            jnp.dot(pick_ref[0], ffn_ref[:, cols], preferred_element_type=F32)
-            .astype(BF16)
-            .reshape(nsp, cap, COLS)
-        )
-        return carry
-
-    lax.fori_loop(0, col_steps, spread, 0)
-
-    def peer(k):
-        away = lax.div(k + 1, 2)
-        return lax.rem(lax.rem(k, 2) * away + (1 - lax.rem(k, 2)) * (nsp - away) + sp, nsp)
-
-    def dispatch(k, carry):
-        to = peer(k)
-        remote(o_ref.at[to], x_ref.at[sp], 10, to, tp).start()
-        return carry
-
-    lax.fori_loop(1, nsp, dispatch, 0)
-    x_ref[sp] = o_ref[sp]
-
-    got(e_ref.at[:, 0, pl.ds(0, nx - 1), 0], 8)
-    for k in range(1, ny):
-        ref = e_ref.at[:, my_y, :, 0]
-        remote(ref, ref, 11, sp, tp_at(my_y + k, my_x)).start()
-    got(e_ref.at[:, pl.ds(0, ny - 1), 0, 1], 9)
-    for k in range(1, nx):
-        ref = e_ref.at[:, :, my_x, 1]
-        remote(ref, ref, 12, sp, tp_at(my_y, my_x + k)).start()
-
-    got(e_ref.at[:, pl.ds(0, ny - 1), :, 0], 11)
-    got(e_ref.at[:, :, pl.ds(0, nx - 1), 1], 12)
-    got(x_ref.at[pl.ds(0, nsp - 1)], 10)
+    spread(ffn_ref, on_ref)
+    send_blocks(on_ref, x_ref, 10, 1, far - 1)
+    send_block(on_ref, x_ref, 10, far, far - 1)
+    x_ref[0] = on_ref[sp]
+
+    got(e_ref.at[:, pl.ds(0, min(2, ny - 1)), :, 0], 11)
+    if ny > 2:
+        before, after = lax.rem(my_y + ny - 1, ny), lax.rem(my_y + 1, ny)
+        ref = e_ref.at[:, before, :, 0, :, pl.ds(0, width // 2)]
+        remote(ref, ref, 16, sp, tp_at(after, my_x)).start()
+        ref = e_ref.at[:, after, :, 0, :, pl.ds(width // 2, width // 2)]
+        remote(ref, ref, 16, sp, tp_at(before, my_x)).start()
+    got(e_ref.at[:, :, pl.ds(0, min(2, nx - 1)), 1], 12)
+    if nx > 2:
+        before, after = lax.rem(my_x + nx - 1, nx), lax.rem(my_x + 1, nx)
+        ref = e_ref.at[:, :, before, 1, :, pl.ds(0, width // 2)]
+        remote(ref, ref, 17, sp, tp_at(my_y, after)).start()
+        ref = e_ref.at[:, :, after, 1, :, pl.ds(width // 2, width // 2)]
+        remote(ref, ref, 17, sp, tp_at(my_y, before)).start()
+    if ny > 2:
+        got(e_ref.at[:, 0, :, 0], 16)
+    if nx > 2:
+        got(e_ref.at[:, :, 0, 1], 17)
 
     per_y = nx * 32
     nt = (((1,), (1,)), ((), ()))
-
-    def expert_in(index, carry):
-        ys = pl.ds(index * 2, 2)
-        arriving = x_ref[...].reshape(slots, width)
-        gate_rows = e_ref[0, ys].reshape(2 * per_y, width)
-        up_rows = e_ref[1, ys].reshape(2 * per_y, width)
-        gate_vals = lax.dot_general(arriving, gate_rows, nt, preferred_element_type=F32)
-        up_vals = lax.dot_general(arriving, up_rows, nt, preferred_element_type=F32)
-        hid_ref[index] = (gate_vals * jax.nn.sigmoid(gate_vals) * up_vals).astype(BF16)
-        return carry
-
-    lax.fori_loop(0, ny // 2, expert_in, 0)
-
-    def expert_out(index, carry):
+    sources = max(16 // cap, 1)
+
+    def rows_at(index):
+        count = sources * cap
+        return pl.ds(pl.multiple_of(index * count, count), count)
+
+    def blocks_at(base, index):
+        return x_ref[pl.ds(base + index * sources, sources)].reshape(sources * cap, width)
+
+    def serve(base, end):
+        rows = (end - base) * cap
+
+        def expert_in(index, carry):
+            ys = pl.ds(index * 2, 2)
+            gate_rows = e_ref[0, ys].reshape(2 * per_y, width)
+            up_rows = e_ref[1, ys].reshape(2 * per_y, width)
+            inputs = xf_ref[0:rows, :]
+            gate_vals = lax.dot_general(inputs, gate_rows, nt, preferred_element_type=F32)
+            up_vals = lax.dot_general(inputs, up_rows, nt, preferred_element_type=F32)
+            hid_ref[index, 0:rows, :] = (
+                gate_vals * jax.nn.sigmoid(gate_vals) * up_vals
+            ).astype(BF16)
+            return carry
+
+        lax.fori_loop(0, ny // 2, expert_in, 0)
+
+        def expert_out(index, carry):
+            cols = cols_of(index)
+            total = None
+            for pair in range(ny // 2):
+                down = e_ref[2, 2 * pair : 2 * pair + 2, :, :, :, cols].reshape(2 * per_y, COLS)
+                product = jnp.dot(hid_ref[pair, 0:rows, :], down, preferred_element_type=F32)
+                total = product if total is None else total + product
+            y_ref[base:end, :, cols] = total.astype(BF16).reshape(end - base, cap, COLS)
+            return carry
+
+        lax.fori_loop(0, col_steps, expert_out, 0)
+
+        def give_back(k, carry):
+            remote(y_ref.at[k], r_ref.at[sp], 13, peer(k), tp).start()
+            return carry
+
+        lax.fori_loop(max(base, 1), end, give_back, 0)
+
+    got(x_ref.at[pl.ds(0, nsp - far)], 14)
+    got(xb_ref, 15)
+
+    def mix_arrived(index, carry):
         cols = cols_of(index)
-        total = None
-        for half in range(ny // 2):
-            down = e_ref[2, 2 * half : 2 * half + 2, :, :, :, cols].reshape(2 * per_y, COLS)
-            part = jnp.dot(hid_ref[half], down, preferred_element_type=F32)
-            total = part if total is None else total + part
-        y_ref[:, :, cols] = total.astype(BF16).reshape(nsp, cap, COLS)
-        return carry
-
-    lax.fori_loop(0, col_steps, expert_out, 0)
-
-    def give_back(k, carry):
-        to = peer(k)
-        remote(y_ref.at[to], r_ref.at[sp], 13, to, tp).start()
-        return carry
-
-    lax.fori_loop(1, nsp, give_back, 0)
-    r_ref[sp] = y_ref[sp]
+        m_ref[:, cols] = jnp.dot(
+            xb_ref[...].reshape((nsp - far) * cap, ntp * chan), projection(cols),
+            preferred_element_type=F32,
+        )
+        return carry
+
+    lax.fori_loop(0, col_steps, mix_arrived, 0)
+
+    def norm_arrived(index, carry):
+        rows = rows_at(index)
+        mixed = m_ref[rows, :]
+        after = (
+            blocks_at(far, index).astype(F32) + mixed * scale(mixed) * gmix_ref[...]
+        )
+        xf_ref[rows, :] = (after * scale(after) * gpre_ref[...]).astype(BF16)
+        return carry
+
+    lax.fori_loop(0, (nsp - far) // sources, norm_arrived, 0)
+    serve(far, nsp)
+
+    got(x_ref.at[pl.ds(0, far - 1)], 10)
+
+    def take_arrived(index, carry):
+        xf_ref[rows_at(index), :] = blocks_at(0, index)
+        return carry
+
+    lax.fori_loop(0, far // sources, take_arrived, 0)
+    serve(0, far)
+    r_ref[sp] = y_ref[0]
     got(r_ref.at[pl.ds(0, nsp - 1)], 13)
 
     def combine(index, carry):
@@ -472,9 +600,15 @@
     sent(w_ref.at[:, :, pl.ds(0, 2)], 7)
     sent(e_ref.at[:, 0, pl.ds(0, nx - 1), 0], 8)
     sent(e_ref.at[:, pl.ds(0, ny - 1), 0, 1], 9)
-    sent(x_ref.at[pl.ds(0, nsp - 1)], 10)
-    sent(e_ref.at[:, pl.ds(0, ny - 1), :, 0], 11)
-    sent(e_ref.at[:, :, pl.ds(0, nx - 1), 1], 12)
+    sent(x_ref.at[pl.ds(0, far - 1)], 10)
+    sent(x_ref.at[pl.ds(0, nsp - far)], 14)
+    sent(xb_ref, 15)
+    sent(e_ref.at[:, pl.ds(0, min(2, ny - 1)), :, 0], 11)
+    if ny > 2:
+        sent(e_ref.at[:, 0, :, 0], 16)
+    sent(e_ref.at[:, :, pl.ds(0, min(2, nx - 1)), 1], 12)
+    if nx > 2:
+        sent(e_ref.at[:, :, 0, 1], 17)
     sent(r_ref.at[pl.ds(0, nsp - 1)], 13)
 
 
@@ -493,12 +627,13 @@
         blocks = positions // LANES
         cap = 2 * toks // nsp
         vmem = pl.BlockSpec(memory_space=pltpu.VMEM)
-        hbm = pl.BlockSpec(memory_space=pl.ANY)
+        hbm = pl.BlockSpec(memory_space=pltpu.HBM)
         block = (blocks, chan, LANES)
+        far = nsp * FAR // 32
         return pl.pallas_call(
             functools.partial(kernel, (nsp, nx, ny)),
             out_shape=jax.ShapeDtypeStruct((toks, width), BF16),
-            in_specs=[hbm] + [vmem] * 7 + [hbm] + [vmem] * 5 + [hbm] * 3,
+            in_specs=[hbm] * 17,
             out_specs=vmem,
             scratch_shapes=[
                 pltpu.VMEM((toks, width), BF16),
@@ -519,16 +654,33 @@
                 pltpu.VMEM((3, nsp * cap, toks), BF16),
                 pltpu.VMEM((nsp, cap, width), BF16),
                 pltpu.VMEM((nsp, cap, width), BF16),
-                pltpu.VMEM((ny // 2, nsp * cap, nx * 64), BF16),
+                pltpu.VMEM((nsp, cap, width), BF16),
+                pltpu.VMEM((nsp, cap, ntp * chan), BF16),
+                pltpu.VMEM((nsp - far, cap, ntp * chan), BF16),
+                pltpu.VMEM(((nsp - far) * cap, width), F32),
+                pltpu.VMEM((max(far, nsp - far) * cap, width), BF16),
+                pltpu.VMEM((ny // 2, max(far, nsp - far) * cap, nx * 64), BF16),
                 pltpu.VMEM((nsp, cap, width), BF16),
                 pltpu.VMEM((nsp, cap, width), BF16),
                 pltpu.VMEM((toks, width), F32),
-                pltpu.SemaphoreType.DMA((5,)),
-                pltpu.SemaphoreType.DMA((14,)),
-                pltpu.SemaphoreType.DMA((14,)),
+                pltpu.VMEM((chan, positions), BF16),
+                pltpu.VMEM((chan, positions), BF16),
+                pltpu.VMEM(conv_taps.shape, BF16),
+                pltpu.VMEM((chan, chan), BF16),
+                pltpu.VMEM((chan, chan), BF16),
+                pltpu.VMEM((1, chan), F32),
+                pltpu.VMEM((blocks, LANES), F32),
+                pltpu.VMEM((1, width), F32),
+                pltpu.VMEM((1, width), F32),
+                pltpu.VMEM((1, width), F32),
+                pltpu.VMEM((2, toks), jnp.int32),
+                pltpu.VMEM((2, toks), F32),
+                pltpu.SemaphoreType.DMA((17,)),
+                pltpu.SemaphoreType.DMA((18,)),
+                pltpu.SemaphoreType.DMA((18,)),
             ],
             compiler_params=pltpu.CompilerParams(
-                collective_id=0, has_side_effects=True, vmem_limit_bytes=52 * 1024 * 1024
+                collective_id=0, has_side_effects=True, vmem_limit_bytes=67043328
             ),
         )(
             resid, branch_input, gate_in, conv_taps,

time: 163 us -> 138 us (0.85)
  the two profiles are of different devices: /device:TPU:36 before, /device:TPU:1 now
where the time goes in v2:
time: 138 us; the launch traced here: 137 us
  Pallas kernels  135 us (98%)
  local copies, waits for them, and re-layouts  1.88 us (1%)
    pallas_call x1, Pallas kernels, per_device(): pl.pallas_call(functools.partial(kernel, (nsp, nx, ny)), out_shape=jax.Sh...  135 us

profile of v2, /device:TPU:1, one launch (start us, length us, event | category | flops | bytes accessed | tf_op | source)
XLA Modules:
  0.0 137.0 jit_solution(15771542979264959211)
XLA Ops:
  0.0 135.1 %shard_map.163 = bf16[128,2048]{1,0:T(8,128)(2,1)} custom-call(bf16[128,2048]{1,0:T(8,128)(2,1)} %resid_hbm.1, bf16[64,2048]{1,0:T(8,128)(2,1)} %branch_hbm.1, bf16[64,2048]{1,0:T(8,128)(2,1)} %gate_hbm.1, bf16[4,64]{1,0:T(4,128)(2,1)} %taps_hbm.1, bf16[64,64]{1,0:T(8,128)(2,1)} %bitcast.17, bf16[64,64]{1,0:T(8,128)(2,1)} %bitcast.18, f32[1,64]{1,0:T(1,128)} %bitcast.25, ...), custom_call_target="tpu_custom_call" | custom-call | tf_op jit(solution)/shard_map/pallas_call | solution.py:633
  135.1 1.9 %copy.19 = bf16[128,2048]{1,0:T(8,128)(2,1)} copy(bf16[128,2048]{1,0:T(8,128)(2,1)} %shard_map.163) | data formatting | bytes 1048576

commit v3 on v2

--- a/solution.py
+++ b/solution.py
@@ -17,7 +17,9 @@
 LANES = 128
 COLS = 512
 GROUP = 4
-FAR = 22
+FAR = 20
+FAR_EDGE = "far"
+NEAR_EDGE = "near"
 
 
 def one_minus_exp(y):
@@ -239,6 +241,7 @@
         return carry
 
     lax.fori_loop(1, blocks // group, later_group, 0)
+    block_group(1, group - 1, branch_ref[:, lanes_of(0)].astype(F32))
 
     for copy in small[6:]:
         copy.wait()
@@ -298,8 +301,16 @@
         away = lax.div(k + 1, 2)
         return lax.rem(lax.rem(k, 2) * away + (1 - lax.rem(k, 2)) * (nsp - away) + sp, nsp)
 
+    if (far // 2) % 4 == 2:
+        reach = nsp - far // 2 + lax.rem(lax.div(sp, 2), 2) * far
+        ahead, behind = lax.rem(sp + nsp - reach + nsp, nsp), lax.rem(sp + reach, nsp)
+        from_far, from_near = ahead, behind
+    else:
+        ahead, behind = peer(far - 1), peer(far)
+        from_far, from_near = behind, ahead
+
     def send_block(source, target, sem, k, place):
-        to = peer(k)
+        to = ahead if k is FAR_EDGE else behind if k is NEAR_EDGE else peer(k)
         remote(source.at[to], target.at[place], sem, to, tp).start()
 
     def send_blocks(source, target, sem, begin, end, offset=0):
@@ -316,7 +327,7 @@
         branch_ref.at[:, pl.ds(positions - LANES, LANES)], halo_ref, 0, lax.rem(sp + 1, nsp), tp
     ).start()
 
-    send_block(o_ref, x_ref, 14, far - 1, far)
+    send_block(o_ref, x_ref, 14, FAR_EDGE, far)
     send_blocks(o_ref, x_ref, 14, far + 1, first_batch)
 
     own[0].wait()
@@ -342,7 +353,7 @@
         remote(ref, ref, 9, sp, tp_at(my_y + k, my_x)).start()
 
     got(halo_ref, 0)
-    block_group(0, group, jnp.where(sp == 0, 0.0, halo_ref[...].astype(F32)))
+    block_group(0, 1, jnp.where(sp == 0, 0.0, halo_ref[...].astype(F32)))
 
     def chain(index, carry):
         keep, state = carry
@@ -369,36 +380,6 @@
     send_blocks(o_ref, x_ref, 14, first_batch, nsp - 1)
     send_block(o_ref, x_ref, 14, nsp - 1, nsp - 1)
 
-    got(sums_ref.at[pl.ds(0, nsp - 1)], 5)
-
-    def fold(index, carry):
-        line = sums_ref[index]
-        keep = jnp.where(index < sp, to_column(line, chan), 1.0)
-        moved = jnp.where(
-            index < sp,
-            jnp.sum(jnp.where(lane == row + chan, line, 0.0), axis=1, keepdims=True),
-            0.0,
-        )
-        return keep * carry + moved
-
-    entering = lax.fori_loop(0, nsp, fold, jnp.zeros((chan, 1), F32), unroll=True)
-
-    def finish(index, carry):
-        begin = last_state[index] + last_keep[index] * entering
-        hidden = state_ref[index] + keep_ref[index] * begin
-        bo_ref[index] = (hidden * act_ref[index]).astype(BF16)
-        return carry
-
-    lax.fori_loop(0, blocks, finish, 0)
-
-    def send_tokens(k, carry):
-        to = lax.rem(tp + k, ntp)
-        remote(bo_ref.at[to], tok_ref.at[tp], 6, sp, to).start()
-        return carry
-
-    lax.fori_loop(1, ntp, send_tokens, 0)
-    tok_ref[tp] = bo_ref[tp]
-
     got(w_ref.at[0, pl.ds(0, nx - 1), 0], 1)
     for k in range(1, ny):
         ref = w_ref.at[my_y, :, half_a]
@@ -408,14 +389,50 @@
         ref = w_ref.at[:, my_x, half_b]
         remote(ref, ref, 4, sp, tp_at(my_y, my_x + k)).start()
 
+    got(sums_ref.at[pl.ds(0, nsp - 1)], 5)
+
+    def fold(index, carry):
+        line = sums_ref[index]
+        keep = jnp.where(index < sp, to_column(line, chan), 1.0)
+        moved = jnp.where(
+            index < sp,
+            jnp.sum(jnp.where(lane == row + chan, line, 0.0), axis=1, keepdims=True),
+            0.0,
+        )
+        return keep * carry + moved
+
+    entering = lax.fori_loop(0, nsp, fold, jnp.zeros((chan, 1), F32), unroll=True)
+
+    def finish(index, carry):
+        begin = last_state[index] + last_keep[index] * entering
+        hidden = state_ref[index] + keep_ref[index] * begin
+        bo_ref[index] = (hidden * act_ref[index]).astype(BF16)
+        return carry
+
+    lax.fori_loop(0, blocks, finish, 0)
+
+    def send_tokens(k, carry):
+        to = lax.rem(tp + k, ntp)
+        remote(bo_ref.at[to], tok_ref.at[tp], 6, sp, to).start()
+        return carry
+
+    lax.fori_loop(1, ntp, send_tokens, 0)
+    tok_ref[tp] = bo_ref[tp]
+
     got(e_ref.at[:, 0, pl.ds(0, nx - 1), 0], 8)
-    for k in sorted({1, ny - 1}):
-        ref = e_ref.at[:, my_y, :, 0]
-        remote(ref, ref, 11, sp, tp_at(my_y + k, my_x)).start()
     got(e_ref.at[:, pl.ds(0, ny - 1), 0, 1], 9)
-    for k in sorted({1, nx - 1}):
-        ref = e_ref.at[:, :, my_x, 1]
-        remote(ref, ref, 12, sp, tp_at(my_y, my_x + k)).start()
+    for a in range(3):
+        for k in sorted({1, ny - 1}):
+            ref = e_ref.at[a, my_y, :, 0]
+            remote(ref, ref, 18 + a, sp, tp_at(my_y + k, my_x)).start()
+        for k in sorted({1, nx - 1}):
+            ref = e_ref.at[a, :, my_x, 1]
+            remote(ref, ref, 21 + a, sp, tp_at(my_y, my_x + k)).start()
+
+    got(w_ref.at[pl.ds(0, ny - 1), :, 0], 3)
+    got(w_ref.at[:, pl.ds(0, nx - 1), 0], 4)
+    ref = w_ref.at[:, :, pl.ds(2 * core, 2)]
+    remote(ref, ref, 7, sp + 1 - 2 * core, tp).start()
 
     got(tok_ref.at[pl.ds(0, ntp - 1)], 6)
     ob_ref[...] = (
@@ -426,14 +443,10 @@
         .astype(BF16)
         .reshape(nsp, cap, ntp * chan)
     )
-    send_block(ob_ref, xb_ref, 15, far - 1, 0)
+    send_block(ob_ref, xb_ref, 15, FAR_EDGE, 0)
     send_blocks(ob_ref, xb_ref, 15, far + 1, nsp - 1, far)
     send_block(ob_ref, xb_ref, 15, nsp - 1, nsp - 1 - far)
 
-    got(w_ref.at[pl.ds(0, ny - 1), :, 0], 3)
-    got(w_ref.at[:, pl.ds(0, nx - 1), 0], 4)
-    ref = w_ref.at[:, :, pl.ds(2 * core, 2)]
-    remote(ref, ref, 7, sp + 1 - 2 * core, tp).start()
     got(w_ref.at[:, :, pl.ds(0, 2)], 7)
 
     def scale(values):
@@ -463,31 +476,36 @@
         ffn_ref[rows, :] = (after * scale(after) * gpre_ref[...]).astype(BF16)
         return carry
 
-    lax.fori_loop(0, toks // 16, norms, 0)
+    lax.fori_loop(0, toks // 16, norms, 0, unroll=2)
 
     spread(ffn_ref, on_ref)
     send_blocks(on_ref, x_ref, 10, 1, far - 1)
-    send_block(on_ref, x_ref, 10, far, far - 1)
+    send_block(on_ref, x_ref, 10, NEAR_EDGE, far - 1)
     x_ref[0] = on_ref[sp]
 
-    got(e_ref.at[:, pl.ds(0, min(2, ny - 1)), :, 0], 11)
-    if ny > 2:
-        before, after = lax.rem(my_y + ny - 1, ny), lax.rem(my_y + 1, ny)
-        ref = e_ref.at[:, before, :, 0, :, pl.ds(0, width // 2)]
-        remote(ref, ref, 16, sp, tp_at(after, my_x)).start()
-        ref = e_ref.at[:, after, :, 0, :, pl.ds(width // 2, width // 2)]
-        remote(ref, ref, 16, sp, tp_at(before, my_x)).start()
-    got(e_ref.at[:, :, pl.ds(0, min(2, nx - 1)), 1], 12)
-    if nx > 2:
-        before, after = lax.rem(my_x + nx - 1, nx), lax.rem(my_x + 1, nx)
-        ref = e_ref.at[:, :, before, 1, :, pl.ds(0, width // 2)]
-        remote(ref, ref, 17, sp, tp_at(my_y, after)).start()
-        ref = e_ref.at[:, :, after, 1, :, pl.ds(width // 2, width // 2)]
-        remote(ref, ref, 17, sp, tp_at(my_y, before)).start()
-    if ny > 2:
-        got(e_ref.at[:, 0, :, 0], 16)
-    if nx > 2:
-        got(e_ref.at[:, :, 0, 1], 17)
+    near_y, near_x = min(2, ny - 1), min(2, nx - 1)
+    low, high = pl.ds(0, width // 2), pl.ds(width // 2, width // 2)
+    for a in range(3):
+        got(e_ref.at[a, pl.ds(0, near_y), :, 0], 18 + a)
+        if ny > 2:
+            before, after = lax.rem(my_y + ny - 1, ny), lax.rem(my_y + 1, ny)
+            ref = e_ref.at[a, before, :, 0, :, low]
+            remote(ref, ref, 24 + a, sp, tp_at(after, my_x)).start()
+            ref = e_ref.at[a, after, :, 0, :, high]
+            remote(ref, ref, 24 + a, sp, tp_at(before, my_x)).start()
+        got(e_ref.at[a, :, pl.ds(0, near_x), 1], 21 + a)
+        if nx > 2:
+            before, after = lax.rem(my_x + nx - 1, nx), lax.rem(my_x + 1, nx)
+            ref = e_ref.at[a, :, before, 1, :, low]
+            remote(ref, ref, 27 + a, sp, tp_at(my_y, after)).start()
+            ref = e_ref.at[a, :, after, 1, :, high]
+            remote(ref, ref, 27 + a, sp, tp_at(my_y, before)).start()
+
+    def whole_weights(a):
+        if ny > 2:
+            got(e_ref.at[a, 0, :, 0], 24 + a)
+        if nx > 2:
+            got(e_ref.at[a, :, 0, 1], 27 + a)
 
     per_y = nx * 32
     nt = (((1,), (1,)), ((), ()))
@@ -500,8 +518,11 @@
     def blocks_at(base, index):
         return x_ref[pl.ds(base + index * sources, sources)].reshape(sources * cap, width)
 
-    def serve(base, end):
+    def serve(base, end, first):
         rows = (end - base) * cap
+        if first:
+            whole_weights(0)
+            whole_weights(1)
 
         def expert_in(index, carry):
             ys = pl.ds(index * 2, 2)
@@ -517,6 +538,9 @@
 
         lax.fori_loop(0, ny // 2, expert_in, 0)
 
+        if first:
+            whole_weights(2)
+
         def expert_out(index, carry):
             cols = cols_of(index)
             total = None
@@ -533,7 +557,12 @@
             remote(y_ref.at[k], r_ref.at[sp], 13, peer(k), tp).start()
             return carry
 
-        lax.fori_loop(max(base, 1), end, give_back, 0)
+        if first:
+            lax.fori_loop(far + 1, nsp, give_back, 0)
+            remote(y_ref.at[far], r_ref.at[sp], 13, from_far, tp).start()
+        else:
+            lax.fori_loop(1, far - 1, give_back, 0)
+            remote(y_ref.at[far - 1], r_ref.at[sp], 13, from_near, tp).start()
 
     got(x_ref.at[pl.ds(0, nsp - far)], 14)
     got(xb_ref, 15)
@@ -557,8 +586,8 @@
         xf_ref[rows, :] = (after * scale(after) * gpre_ref[...]).astype(BF16)
         return carry
 
-    lax.fori_loop(0, (nsp - far) // sources, norm_arrived, 0)
-    serve(far, nsp)
+    lax.fori_loop(0, (nsp - far) // sources, norm_arrived, 0, unroll=2)
+    serve(far, nsp, True)
 
     got(x_ref.at[pl.ds(0, far - 1)], 10)
 
@@ -567,7 +596,7 @@
         return carry
 
     lax.fori_loop(0, far // sources, take_arrived, 0)
-    serve(0, far)
+    serve(0, far, False)
     r_ref[sp] = y_ref[0]
     got(r_ref.at[pl.ds(0, nsp - 1)], 13)
 
@@ -588,7 +617,7 @@
         out_ref[rows, :] = (after_ref[rows, :] + moe * scale(moe) * gpost_ref[...]).astype(BF16)
         return carry
 
-    lax.fori_loop(0, toks // 16, finalize, 0)
+    lax.fori_loop(0, toks // 16, finalize, 0, unroll=2)
 
     sent(halo_ref, 0)
     sent(w_ref.at[0, pl.ds(0, nx - 1), 0], 1)
@@ -603,12 +632,13 @@
     sent(x_ref.at[pl.ds(0, far - 1)], 10)
     sent(x_ref.at[pl.ds(0, nsp - far)], 14)
     sent(xb_ref, 15)
-    sent(e_ref.at[:, pl.ds(0, min(2, ny - 1)), :, 0], 11)
-    if ny > 2:
-        sent(e_ref.at[:, 0, :, 0], 16)
-    sent(e_ref.at[:, :, pl.ds(0, min(2, nx - 1)), 1], 12)
-    if nx > 2:
-        sent(e_ref.at[:, :, 0, 1], 17)
+    for a in range(3):
+        sent(e_ref.at[a, pl.ds(0, near_y), :, 0], 18 + a)
+        sent(e_ref.at[a, :, pl.ds(0, near_x), 1], 21 + a)
+        if ny > 2:
+            sent(e_ref.at[a, 0, :, 0], 24 + a)
+        if nx > 2:
+            sent(e_ref.at[a, :, 0, 1], 27 + a)
     sent(r_ref.at[pl.ds(0, nsp - 1)], 13)
 
 
@@ -676,8 +706,8 @@
                 pltpu.VMEM((2, toks), jnp.int32),
                 pltpu.VMEM((2, toks), F32),
                 pltpu.SemaphoreType.DMA((17,)),
-                pltpu.SemaphoreType.DMA((18,)),
-                pltpu.SemaphoreType.DMA((18,)),
+                pltpu.SemaphoreType.DMA((30,)),
+                pltpu.SemaphoreType.DMA((30,)),
             ],
             compiler_params=pltpu.CompilerParams(
                 collective_id=0, has_side_effects=True, vmem_limit_bytes=67043328

time: 138 us -> 133 us (0.964)
  Pallas kernels: 135 us -> 131 us
    pallas_call x1, Pallas kernels: 135 us -> 131 us  [per_device(): pl.pallas_call(functools.partial(kernel, (nsp, nx, ny)), out_shape=jax.Sh...]
where the time goes in v3:
time: 133 us
  Pallas kernels  131 us (98%)
  local copies, waits for them, and re-layouts  1.88 us (1%)
    pallas_call x1, Pallas kernels, per_device(): pl.pallas_call(functools.partial(kernel, (nsp, nx, ny)), out_shape=jax.Sh...  131 us

profile of v3, /device:TPU:1, one launch (start us, length us, event | category | flops | bytes accessed | tf_op | source)
XLA Modules:
  0.0 133.1 jit_solution(12297402880363049480)
XLA Ops:
  0.0 131.2 %shard_map.163 = bf16[128,2048]{1,0:T(8,128)(2,1)} custom-call(bf16[128,2048]{1,0:T(8,128)(2,1)} %resid_hbm.1, bf16[64,2048]{1,0:T(8,128)(2,1)} %branch_hbm.1, bf16[64,2048]{1,0:T(8,128)(2,1)} %gate_hbm.1, bf16[4,64]{1,0:T(4,128)(2,1)} %taps_hbm.1, bf16[64,64]{1,0:T(8,128)(2,1)} %bitcast.17, bf16[64,64]{1,0:T(8,128)(2,1)} %bitcast.18, f32[1,64]{1,0:T(1,128)} %bitcast.25, ...), custom_call_target="tpu_custom_call" | custom-call | tf_op jit(solution)/shard_map/pallas_call | solution.py:663
  131.2 1.9 %copy.19 = bf16[128,2048]{1,0:T(8,128)(2,1)} copy(bf16[128,2048]{1,0:T(8,128)(2,1)} %shard_map.163) | data formatting | bytes 1048576

commit v4 on v3

--- a/solution.py
+++ b/solution.py
@@ -17,7 +17,7 @@
 LANES = 128
 COLS = 512
 GROUP = 4
-FAR = 20
+FAR = 22
 FAR_EDGE = "far"
 NEAR_EDGE = "near"
 
@@ -137,6 +137,23 @@
     def sent(ref, k):
         pltpu.make_async_copy(ref, ref, send_sem.at[k]).wait()
 
+    barrier = pltpu.get_barrier_semaphore()
+
+    def greet_sp(k, carry):
+        pl.semaphore_signal(
+            barrier, inc=1, device_id=(lax.rem(sp + k, nsp), tp), device_id_type=MESH
+        )
+        return carry
+
+    def greet_tp(k, carry):
+        pl.semaphore_signal(
+            barrier, inc=1, device_id=(sp, lax.rem(tp + k, ntp)), device_id_type=MESH
+        )
+        return carry
+
+    lax.fori_loop(1, nsp, greet_sp, 0)
+    lax.fori_loop(1, ntp, greet_tp, 0)
+
     own = [
         pltpu.make_async_copy(outw_hbm, w_ref.at[my_y, my_x], loc_sem.at[0]),
         pltpu.make_async_copy(gp_hbm, e_ref.at[0, my_y, my_x], loc_sem.at[1]),
@@ -155,23 +172,6 @@
     ]
     for copy in small + own:
         copy.start()
-
-    barrier = pltpu.get_barrier_semaphore()
-
-    def greet_sp(k, carry):
-        pl.semaphore_signal(
-            barrier, inc=1, device_id=(lax.rem(sp + k, nsp), tp), device_id_type=MESH
-        )
-        return carry
-
-    def greet_tp(k, carry):
-        pl.semaphore_signal(
-            barrier, inc=1, device_id=(sp, lax.rem(tp + k, ntp)), device_id_type=MESH
-        )
-        return carry
-
-    lax.fori_loop(1, nsp, greet_sp, 0)
-    lax.fori_loop(1, ntp, greet_tp, 0)
 
     for copy in small[:6]:
         copy.wait()
@@ -240,17 +240,9 @@
         block_group(first, group, branch_ref[:, lanes_of(first - 1)].astype(F32))
         return carry
 
-    lax.fori_loop(1, blocks // group, later_group, 0)
-    block_group(1, group - 1, branch_ref[:, lanes_of(0)].astype(F32))
 
     for copy in small[6:]:
         copy.wait()
-
-    def activate(index, carry):
-        act_ref[index] = gelu(gate_ref[:, lanes_of(index)].astype(F32))
-        return carry
-
-    lax.fori_loop(0, blocks, activate, 0)
 
     ids = ids_ref[...]
     expert = lax.broadcasted_iota(jnp.int32, (nsp, toks), 0)
@@ -322,6 +314,9 @@
 
     first_batch = min(far + 2, nsp - 1)
 
+    early_groups = min(2, blocks // group)
+    lax.fori_loop(early_groups + 1, blocks // group, later_group, 0)
+
     pl.semaphore_wait(barrier, nsp - 1 + ntp - 1)
     remote(
         branch_ref.at[:, pl.ds(positions - LANES, LANES)], halo_ref, 0, lax.rem(sp + 1, nsp), tp
@@ -346,12 +341,14 @@
     for copy in own[1:4]:
         copy.wait()
     for k in range(1, nx):
-        ref = e_ref.at[:, my_y, my_x, 0]
+        ref = e_ref.at[0, my_y, my_x, 0]
         remote(ref, ref, 8, sp, tp_at(my_y, my_x + k)).start()
     for k in range(1, ny):
-        ref = e_ref.at[:, my_y, my_x, 1]
+        ref = e_ref.at[0, my_y, my_x, 1]
         remote(ref, ref, 9, sp, tp_at(my_y + k, my_x)).start()
 
+    lax.fori_loop(1, min(early_groups + 1, blocks // group), later_group, 0)
+    block_group(1, group - 1, branch_ref[:, lanes_of(0)].astype(F32))
     got(halo_ref, 0)
     block_group(0, 1, jnp.where(sp == 0, 0.0, halo_ref[...].astype(F32)))
 
@@ -389,6 +386,12 @@
         ref = w_ref.at[:, my_x, half_b]
         remote(ref, ref, 4, sp, tp_at(my_y, my_x + k)).start()
 
+    def activate(index, carry):
+        act_ref[index] = gelu(gate_ref[:, lanes_of(index)].astype(F32))
+        return carry
+
+    lax.fori_loop(0, blocks, activate, 0)
+
     got(sums_ref.at[pl.ds(0, nsp - 1)], 5)
 
     def fold(index, carry):
@@ -419,9 +422,14 @@
     lax.fori_loop(1, ntp, send_tokens, 0)
     tok_ref[tp] = bo_ref[tp]
 
-    got(e_ref.at[:, 0, pl.ds(0, nx - 1), 0], 8)
-    got(e_ref.at[:, pl.ds(0, ny - 1), 0, 1], 9)
-    for a in range(3):
+    for k in range(1, nx):
+        ref = e_ref.at[pl.ds(1, 2), my_y, my_x, 0]
+        remote(ref, ref, 11, sp, tp_at(my_y, my_x + k)).start()
+    for k in range(1, ny):
+        ref = e_ref.at[pl.ds(1, 2), my_y, my_x, 1]
+        remote(ref, ref, 12, sp, tp_at(my_y + k, my_x)).start()
+
+    def second_leg(a):
         for k in sorted({1, ny - 1}):
             ref = e_ref.at[a, my_y, :, 0]
             remote(ref, ref, 18 + a, sp, tp_at(my_y + k, my_x)).start()
@@ -429,6 +437,10 @@
             ref = e_ref.at[a, :, my_x, 1]
             remote(ref, ref, 21 + a, sp, tp_at(my_y, my_x + k)).start()
 
+    got(e_ref.at[0, 0, pl.ds(0, nx - 1), 0], 8)
+    got(e_ref.at[0, pl.ds(0, ny - 1), 0, 1], 9)
+    second_leg(0)
+
     got(w_ref.at[pl.ds(0, ny - 1), :, 0], 3)
     got(w_ref.at[:, pl.ds(0, nx - 1), 0], 4)
     ref = w_ref.at[:, :, pl.ds(2 * core, 2)]
@@ -483,6 +495,10 @@
     send_block(on_ref, x_ref, 10, NEAR_EDGE, far - 1)
     x_ref[0] = on_ref[sp]
 
+    got(e_ref.at[pl.ds(1, 2), 0, pl.ds(0, nx - 1), 0], 11)
+    got(e_ref.at[pl.ds(1, 2), pl.ds(0, ny - 1), 0, 1], 12)
+    second_leg(1)
+    second_leg(2)
     near_y, near_x = min(2, ny - 1), min(2, nx - 1)
     low, high = pl.ds(0, width // 2), pl.ds(width // 2, width // 2)
     for a in range(3):
@@ -627,8 +643,10 @@
     sent(sums_ref.at[pl.ds(0, nsp - 1)], 5)
     sent(tok_ref.at[pl.ds(0, ntp - 1)], 6)
     sent(w_ref.at[:, :, pl.ds(0, 2)], 7)
-    sent(e_ref.at[:, 0, pl.ds(0, nx - 1), 0], 8)
-    sent(e_ref.at[:, pl.ds(0, ny - 1), 0, 1], 9)
+    sent(e_ref.at[0, 0, pl.ds(0, nx - 1), 0], 8)
+    sent(e_ref.at[0, pl.ds(0, ny - 1), 0, 1], 9)
+    sent(e_ref.at[pl.ds(1, 2), 0, pl.ds(0, nx - 1), 0], 11)
+    sent(e_ref.at[pl.ds(1, 2), pl.ds(0, ny - 1), 0, 1], 12)
     sent(x_ref.at[pl.ds(0, far - 1)], 10)
     sent(x_ref.at[pl.ds(0, nsp - far)], 14)
     sent(xb_ref, 15)

time: 133 us -> 129 us (0.970)
  Pallas kernels: 131 us -> 126 us
    pallas_call x1, Pallas kernels: 131 us -> 126 us  [per_device(): pl.pallas_call(functools.partial(kernel, (nsp, nx, ny)), out_shape=jax.Sh...]
where the time goes in v4:
time: 129 us; the launch traced here: 128 us
  Pallas kernels  126 us (98%)
  local copies, waits for them, and re-layouts  1.88 us (1%)
    pallas_call x1, Pallas kernels, per_device(): pl.pallas_call(functools.partial(kernel, (nsp, nx, ny)), out_shape=jax.Sh...  126 us

profile of v4, /device:TPU:1, one launch (start us, length us, event | category | flops | bytes accessed | tf_op | source)
XLA Modules:
  0.0 128.3 jit_solution(11369470356437797804)
XLA Ops:
  0.0 126.4 %shard_map.163 = bf16[128,2048]{1,0:T(8,128)(2,1)} custom-call(bf16[128,2048]{1,0:T(8,128)(2,1)} %resid_hbm.1, bf16[64,2048]{1,0:T(8,128)(2,1)} %branch_hbm.1, bf16[64,2048]{1,0:T(8,128)(2,1)} %gate_hbm.1, bf16[4,64]{1,0:T(4,128)(2,1)} %taps_hbm.1, bf16[64,64]{1,0:T(8,128)(2,1)} %bitcast.17, bf16[64,64]{1,0:T(8,128)(2,1)} %bitcast.18, f32[1,64]{1,0:T(1,128)} %bitcast.25, ...), custom_call_target="tpu_custom_call" | custom-call | tf_op jit(solution)/shard_map/pallas_call | solution.py:681
  126.4 1.9 %copy.19 = bf16[128,2048]{1,0:T(8,128)(2,1)} copy(bf16[128,2048]{1,0:T(8,128)(2,1)} %shard_map.163) | data formatting | bytes 1048576

commit v5 on v4

--- a/solution.py
+++ b/solution.py
@@ -111,6 +111,7 @@
     loc_sem,
     send_sem,
     recv_sem,
+    out_sem,
 ):
     nsp, nx, ny = cfg
     ntp = nx * ny
@@ -141,7 +142,8 @@
 
     def greet_sp(k, carry):
         pl.semaphore_signal(
-            barrier, inc=1, device_id=(lax.rem(sp + k, nsp), tp), device_id_type=MESH
+            barrier, inc=1, device_id=(lax.rem(sp + lax.rem(k + nsp // 4 - 1, nsp - 1) + 1, nsp), tp),
+            device_id_type=MESH,
         )
         return carry
 
@@ -627,13 +629,24 @@
 
     lax.fori_loop(0, col_steps, combine, 0)
 
+    def put_out(index):
+        rows = rows_of(index)
+        pltpu.make_async_copy(ffn_ref.at[rows, :], out_ref.at[rows, :], out_sem).start()
+
     def finalize(index, carry):
         rows = rows_of(index)
         moe = moe_ref[rows, :]
-        out_ref[rows, :] = (after_ref[rows, :] + moe * scale(moe) * gpost_ref[...]).astype(BF16)
+        ffn_ref[rows, :] = (after_ref[rows, :] + moe * scale(moe) * gpost_ref[...]).astype(BF16)
+
+        @pl.when(index > 0)
+        def _():
+            put_out(index - 1)
+
         return carry
 
     lax.fori_loop(0, toks // 16, finalize, 0, unroll=2)
+
+    put_out(toks // 16 - 1)
 
     sent(halo_ref, 0)
     sent(w_ref.at[0, pl.ds(0, nx - 1), 0], 1)
@@ -658,6 +671,7 @@
         if nx > 2:
             sent(e_ref.at[a, :, 0, 1], 27 + a)
     sent(r_ref.at[pl.ds(0, nsp - 1)], 13)
+    pltpu.make_async_copy(ffn_ref, out_ref, out_sem).wait()
 
 
 def solution(mesh):
@@ -674,7 +688,6 @@
         toks, width = resid.shape
         blocks = positions // LANES
         cap = 2 * toks // nsp
-        vmem = pl.BlockSpec(memory_space=pltpu.VMEM)
         hbm = pl.BlockSpec(memory_space=pltpu.HBM)
         block = (blocks, chan, LANES)
         far = nsp * FAR // 32
@@ -682,7 +695,7 @@
             functools.partial(kernel, (nsp, nx, ny)),
             out_shape=jax.ShapeDtypeStruct((toks, width), BF16),
             in_specs=[hbm] * 17,
-            out_specs=vmem,
+            out_specs=hbm,
             scratch_shapes=[
                 pltpu.VMEM((toks, width), BF16),
                 pltpu.VMEM(block, F32),
@@ -726,6 +739,7 @@
                 pltpu.SemaphoreType.DMA((17,)),
                 pltpu.SemaphoreType.DMA((30,)),
                 pltpu.SemaphoreType.DMA((30,)),
+                pltpu.SemaphoreType.DMA,
             ],
             compiler_params=pltpu.CompilerParams(
                 collective_id=0, has_side_effects=True, vmem_limit_bytes=67043328

time: 129 us -> 129 us (level)
  no operation moved by 1% of the time
where the time goes in v5:
time: 129 us; the launch traced here: 128 us
  Pallas kernels  127 us (98%)
  local copies, waits for them, and re-layouts  1.88 us (1%)
    pallas_call x1, Pallas kernels, per_device(): pl.pallas_call(functools.partial(kernel, (nsp, nx, ny)), out_shape=jax.Sh...  127 us

profile of v5, /device:TPU:1, one launch (start us, length us, event | category | flops | bytes accessed | tf_op | source)
XLA Modules:
  0.0 128.5 jit_solution(14219092850609071818)
XLA Ops:
  0.0 126.6 %shard_map.163 = bf16[128,2048]{1,0:T(8,128)(2,1)} custom-call(bf16[128,2048]{1,0:T(8,128)(2,1)} %resid_hbm.1, bf16[64,2048]{1,0:T(8,128)(2,1)} %branch_hbm.1, bf16[64,2048]{1,0:T(8,128)(2,1)} %gate_hbm.1, bf16[4,64]{1,0:T(4,128)(2,1)} %taps_hbm.1, bf16[64,64]{1,0:T(8,128)(2,1)} %bitcast.17, bf16[64,64]{1,0:T(8,128)(2,1)} %bitcast.18, f32[1,64]{1,0:T(1,128)} %bitcast.25, ...), custom_call_target="tpu_custom_call" | custom-call | tf_op jit(solution)/shard_map/pallas_call | solution.py:694
  126.6 1.9 %copy.19 = bf16[128,2048]{1,0:T(8,128)(2,1)} copy(bf16[128,2048]{1,0:T(8,128)(2,1)} %shard_map.163) | data formatting | bytes 1048576
